TPU v7x, 256 devices: a 8x8x2 block of a 8x8x16 slice. The times are simulated.
256 devices in a mesh: grp: 2 (over z), ep: 64 (over y, x), tp: 2 (over core).
Axes of the slice: x: 8, y: 8, z: 2, core: 2. Of those that a mesh axis runs over, the one named last changes fastest.
The devices are a block of a 8x8x16 slice.
Arguments:
- tokens: bfloat16 [65536, 2048], P(('grp', 'ep'), 'tp'), parts along dimension 0, may hold values from -6 to 6
- norm_gain: float32 [2048], replicated, may hold values from 0.1 to 1.9
- expert_ids: int32 [65536, 2], P(('grp', 'ep')), parts along dimension 0, may hold values from 0 to 63, all different within a row; in each aligned block of 512 rows (0 to 511, 512 to 1023, ...) at most 24 rows name the same one
- route_weights: float32 [65536, 2], P(('grp', 'ep')), parts along dimension 0, may hold values from 0.1 to 1
- gate_weight: bfloat16 [64, 2048, 512], P('ep', None, 'tp'), may hold values from -0.125 to 0.125
- up_weight: bfloat16 [64, 2048, 512], P('ep', None, 'tp'), may hold values from -0.125 to 0.125
- down_weight: bfloat16 [64, 512, 2048], P('ep', None, 'tp'), may hold values from -0.25 to 0.25
Outputs:
- mixed: bfloat16 [65536, 2048], P(('grp', 'ep'), 'tp'), parts along dimension 0
There are 2 independent parts, one for each index of `grp`. A program takes and returns all parts, laid end to end along the dimension named above; an argument that names none is the same for every part. Nothing has to cross between parts.
Inputs may be any that keep to these rules, and one draw needn't show every extreme that they name: `expert_ids`: each token names 2 different experts. Among the 512 tokens of one index of ep (aligned blocks of rows) at most 24 name the same expert, and in some block some expert is named by exactly 24 of them.
All inputs are finite; a program needn't handle non-finite values.
Results may differ from a plain program's by a relative error of at most 0.007.
Values may be sent and summed in bfloat16 or wider, within the bound.
No kernel may reach another device: no remote copies, remote signals or barrier semaphores. Data moves between devices by JAX's collectives and lax.ppermute only.
A program may use at most 64 MiB of HBM per device.

v0:
```python
import jax
import jax.numpy as jnp
from jax import lax
from jax.sharding import PartitionSpec as P


def copy_for_each(array, axis):
    copies = jnp.broadcast_to(array, (lax.axis_size(axis), *array.shape))
    return lax.all_to_all(copies, axis, split_axis=0, concat_axis=0, tiled=True)


def joined_along(pieces, dim):
    lengths = list(pieces.shape[1:])
    lengths[dim] *= pieces.shape[0]
    return jnp.moveaxis(pieces, 0, dim).reshape(lengths)


def collect(array, axis, dim):
    pieces = copy_for_each(array, axis)
    return joined_along(pieces, dim)


def cut_along(array, dim, peers):
    lengths = array.shape
    pieces = array.reshape(*lengths[:dim], peers, lengths[dim] // peers, *lengths[dim + 1 :])
    return jnp.moveaxis(pieces, dim, 0)


def cut_rows(length, count):
    turn = length // count
    if turn >= 8:
        turn -= turn % 8
    return [turn * k for k in range(1, count)]


def cut_exchange(array, axis, pieces, split_dim, concat_dim):
    blocks = cut_along(array, split_dim, lax.axis_size(axis))
    split_at = max(range(1, max(2, blocks.ndim - 1)), key=lambda d: blocks.shape[d])
    finished = []
    for section in jnp.split(blocks, cut_rows(blocks.shape[split_at], pieces), axis=split_at):
        if section.size:
            finished.append(lax.all_to_all(section, axis, split_axis=0, concat_axis=0, tiled=True))
    return joined_along(jnp.concatenate(finished, axis=split_at), concat_dim)


def normalize(rows, norm_gain):
    xf = rows.astype(jnp.float32)
    scale = lax.rsqrt(jnp.mean(xf * xf, axis=-1, keepdims=True) + 1e-06)
    return (xf * scale * norm_gain[None, :]).astype(jnp.bfloat16)


def on_device(tokens, norm_gain, expert_ids, route_weights, gate_weight, up_weight, down_weight):
    tok_rows, half = tokens.shape
    width = half * lax.axis_size("tp")
    experts = lax.axis_size("ep")
    top = expert_ids.shape[1]
    capacity = max(2, (3 * tok_rows * top + 2 * experts - 1) // (2 * experts))
    flat = expert_ids.reshape(-1)
    onehot = (flat[:, None] == jnp.arange(experts, dtype=jnp.int32)[None, :]).astype(jnp.int32)
    earlier = jnp.cumsum(onehot, axis=0) - onehot
    slot = jnp.sum(earlier * onehot, axis=-1)
    position = flat * capacity + slot
    owner = jnp.arange(flat.shape[0], dtype=jnp.int32) // top
    w_gate = gate_weight[0]
    w_up = up_weight[0]
    w_down = down_weight[0]
    send = jnp.zeros((experts * capacity, half), jnp.bfloat16).at[position].set(tokens[owner])
    send = send.reshape(experts, capacity, half)
    received = lax.all_to_all(send, "ep", split_axis=0, concat_axis=0, tiled=True)
    sources = received.shape[0]
    count = received.shape[1]
    whole_rows = lax.all_gather(received, "tp", axis=2, tiled=True)
    rows = normalize(whole_rows.reshape(sources * count, width), norm_gain)
    gate = jnp.dot(rows, w_gate, preferred_element_type=jnp.float32)
    upper = jnp.dot(rows, w_up, preferred_element_type=jnp.float32)
    hidden = (jax.nn.silu(gate) * upper).astype(jnp.bfloat16)
    result = jnp.dot(collect(hidden, "tp", 1), w_down, preferred_element_type=jnp.float32)
    result = result.astype(jnp.bfloat16).reshape(sources, count, half)
    back = cut_exchange(result, "ep", 2, 0, 0)
    picked = back.reshape(experts * capacity, half)[position].astype(jnp.float32)
    picked = picked * route_weights.reshape(-1)[:, None]
    return jnp.sum(picked.reshape(tok_rows, top, half), axis=1).astype(jnp.bfloat16)


def solution(mesh):
    in_specs = (
        P(("grp", "ep"), "tp"),
        P(),
        P(("grp", "ep"), None),
        P(("grp", "ep"), None),
        P("ep", None, "tp"),
        P("ep", None, "tp"),
        P("ep", None, "tp"),
    )
    out_specs = P(("grp", "ep"), "tp")
    return jax.shard_map(
        on_device, mesh=mesh, in_specs=in_specs, out_specs=out_specs, check_vma=False
    )
```

profile of v0, /device:TPU:514, one launch (start us, length us, event | category | flops | bytes accessed | tf_op | source)
XLA Modules:
  0.0 322.8 jit_solution(3808967039707982934)
XLA Ops:
  6.6 0.9 copy.26
  7.5 0.2 eq.29
  7.6 0.2 eq.25
  7.8 0.7 broadcast_multiply_fusion
  8.5 18.0 %reduce-window.6 = s32[64,8,128]{2,1,0:T(8,128)S(1)} reduce-window(s32[64,8,128]{2,1,0:T(8,128)S(1)} %fusion.14, s32[]{:T(128)} %constant.31.clone.1), window={size=1x1x128 pad=0_0x0_0x127_0}, to_apply=%region_0.0 | reduce-window | flops 8323072 | bytes 524292 | tf_op jit(solution)/shard_map/reduce-window
  26.7 0.1 copy.28
  27.1 0.1 copy.25
  27.3 0.2 mul.61
  27.6 14.8 %scatter_custom_fusion = bf16[1536,1024]{1,0:T(8,128)(2,1)} fusion(s32[1024]{0:T(1024)S(1)} %bitcast.53, bf16[512,1024]{1,0:T(8,128)(2,1)S(1)} %copy-done, s32[1024]{0:T(1024)S(1)} %broadcast_clamp_fusion.1, bf16[]{:T(256)} %constant.29.clone.1), kind=kCustom, calls=%fused_computation.13 | custom fusion | bytes 3145730 | tf_op jit(solution)/shard_map/scatter | solution.py:67
  42.3 94.8 %all_to_all.20 = bf16[64,24,1024]{2,1,0:T(8,128)(2,1)} all-to-all(bf16[64,24,1024]{2,1,0:T(8,128)(2,1)} %bitcast.44), channel_id=1, replica_groups=mesh['grp'=2,'ep'=64,'tp'=2] {'ep'}, dimensions={0} | all-to-all | bytes 6291456 | tf_op jit(solution)/shard_map/all_to_all | solution.py:69
  137.2 32.5 %all-gather.2.cloned.1.call-done = bf16[64,24,2048]{2,1,0:T(8,128)(2,1)} async-done(((bf16[64,24,1024]{2,1,0:T(8,128)(2,1)}), bf16[64,24,2048]{2,1,0:T(8,128)(2,1)}) %all-gather.2.cloned.1.call-update) | async-done | bytes 6291472 | tf_op jit(solution)/shard_map/all_gather | solution.py:72
  169.7 4.2 %fusion = f32[64,24]{1,0:T(8,128)S(1)} fusion(bf16[64,24,2048]{2,1,0:T(8,128)(2,1)} %all-gather.2.cloned.1.call-done), kind=kLoop, calls=%fused_computation.5 | loop fusion | flops 9435648 | bytes 6297600 | tf_op jit(solution)/shard_map/reduce_sum | solution.py:48
  173.9 0.3 copy-done.1
  174.3 1.5 fusion.2
  175.8 1.9 fusion.9
  177.7 2.1 fusion.3
  179.8 0.3 copy.30
  180.2 5.1 %all_to_all.21 = bf16[2,1536,256]{1,2,0:T(8,128)(2,1)S(1)} all-to-all(bf16[2,1536,256]{1,2,0:T(8,128)(2,1)S(1)} %broadcast_in_dim.5), channel_id=1, replica_groups=mesh['grp'=2,'ep'=64,'tp'=2] {'tp'}, dimensions={0} | all-to-all | bytes 3145728 | tf_op jit(solution)/shard_map/all_to_all | solution.py:9
  185.3 1.8 convolution_convert_fusion
  187.2 1.7 copy-done.3
  188.8 1.0 split.8
  189.9 13.7 %all-to-all-start.2 = ((bf16[64,1,8,1024]{3,2,1,0:T(8,128)(2,1)}), bf16[64,1,8,1024]{3,2,1,0:T(8,128)(2,1)S(1)}, u32[]{:S(2)}, u32[]{:S(2)}) async-start(bf16[64,1,8,1024]{3,2,1,0:T(8,128)(2,1)} %split.8), calls=%async_computation.2 | async-start | bytes 2097152 | tf_op jit(solution)/shard_map/all_to_all | solution.py:42
  203.6 3.3 %split.9 = bf16[64,1,16,1024]{3,2,1,0:T(8,128)(2,1)} slice(bf16[64,1,24,1024]{3,2,1,0:T(8,128)(2,1)} %bitcast.48), slice={[0:64], [0:1], [8:24], [0:1024]} | slice | bytes 4194304 | tf_op jit(solution)/shard_map/split | solution.py:40
  206.9 25.7 %all-to-all-done.2 = bf16[64,1,8,1024]{3,2,1,0:T(8,128)(2,1)S(1)} async-done(((bf16[64,1,8,1024]{3,2,1,0:T(8,128)(2,1)}), bf16[64,1,8,1024]{3,2,1,0:T(8,128)(2,1)S(1)}, u32[]{:S(2)}, u32[]{:S(2)}) %all-to-all-start.2) | async-done | bytes 1048608 | tf_op jit(solution)/shard_map/all_to_all | solution.py:42
  232.6 1.0 copy-done.2
  233.6 7.9 %all-to-all-start.3 = ((bf16[64,1,16,1024]{3,2,1,0:T(8,128)(2,1)}), bf16[64,1,16,1024]{3,2,1,0:T(8,128)(2,1)S(1)}, u32[]{:S(2)}, u32[]{:S(2)}) async-start(bf16[64,1,16,1024]{3,2,1,0:T(8,128)(2,1)} %split.9), calls=%async_computation.3 | async-start | bytes 4194304 | tf_op jit(solution)/shard_map/all_to_all | solution.py:42
  241.6 0.1 copy.33
  241.7 51.0 %all-to-all-done.3 = bf16[64,1,16,1024]{3,2,1,0:T(8,128)(2,1)S(1)} async-done(((bf16[64,1,16,1024]{3,2,1,0:T(8,128)(2,1)}), bf16[64,1,16,1024]{3,2,1,0:T(8,128)(2,1)S(1)}, u32[]{:S(2)}, u32[]{:S(2)}) %all-to-all-start.3) | async-done | bytes 2097184 | tf_op jit(solution)/shard_map/all_to_all | solution.py:42
  292.7 3.3 %pad_maximum_fusion = bf16[64,1,24,1024]{3,2,1,0:T(8,128)(2,1)} fusion(bf16[64,1,16,1024]{3,2,1,0:T(8,128)(2,1)S(1)} %all-to-all-done.3, bf16[64,1,8,1024]{3,2,1,0:T(8,128)(2,1)} %copy-done.2), kind=kLoop, calls=%fused_computation.10 | loop fusion | flops 6291456 | bytes 6291456 | tf_op jit(solution)/shard_map/concatenate | solution.py:43
  296.0 7.3 %gather_fusion = bf16[1024,1024]{1,0:T(8,128)(2,1)S(1)} fusion(bf16[1536,1024]{1,0:T(8,128)(2,1)} %bitcast.43, s32[1024]{0:T(1024)S(1)} %broadcast_clamp_fusion), kind=kCustom, calls=%fused_computation.1 | custom fusion | bytes 4198400 | tf_op jit(solution)/shard_map/gather | solution.py:80
  303.3 4.0 %reshape.142 = f32[512,2,1024]{2,1,0:T(2,128)} reshape(bf16[1024,1024]{1,0:T(8,128)(2,1)S(1)} %gather_fusion) | data formatting | bytes 6291456 | tf_op jit(solution)/shard_map/convert_element_type | solution.py:80
  307.3 8.6 %multiply_reduce_fusion = bf16[512,1024]{1,0:T(8,128)(2,1)} fusion(f32[512,2,1024]{2,1,0:T(2,128)} %reshape.142, f32[512,2]{1,0:T(8,128)S(1)} %copy.33), kind=kLoop, calls=%fused_computation.8 | loop fusion | flops 1572864 | bytes 5246976 | tf_op jit(solution)/shard_map/reduce_sum | solution.py:82
  (30 shorter events, 0.7 us)
Async XLA Ops:
  6.5 21.0 %copy-start = (bf16[512,1024]{1,0:T(8,128)(2,1)S(1)}, bf16[512,1024]{1,0:T(8,128)(2,1)}, u32[]{:S(2)}) copy-start(bf16[512,1024]{1,0:T(8,128)(2,1)} %param.7) | copy-start | bytes 3145732
  6.6 163.1 %all-gather.2.cloned.1.call-start = ((), (), s32[]{:S(2)}) async-start(), calls=%async_computation.4 | async-start | bytes 9437184 | tf_op jit(solution)/shard_map/all_gather | solution.py:72
  137.2 36.7 %copy-start.4 = (f32[2048]{0:T(1024)S(1)}, f32[2048]{0:T(1024)}, u32[]{:S(2)}) copy-start(f32[2048]{0:T(1024)} %param.8) | copy-start | bytes 24580
  169.7 4.6 %copy-start.1 = (bf16[64,24,2048]{2,1,0:T(8,128)(2,1)S(1)}, bf16[64,24,2048]{2,1,0:T(8,128)(2,1)}, u32[]{:S(2)}) copy-start(bf16[64,24,2048]{2,1,0:T(8,128)(2,1)} %all-gather.2.cloned.1.call-done) | copy-start | bytes 18874372
  174.3 1.5 copy-start.6
  175.8 1.9 copy-start.7
  180.0 5.3 %copy-start.8 = (bf16[1,512,1024]{2,1,0:T(8,128)(2,1)S(1)}, bf16[1,512,1024]{2,1,0:T(8,128)(2,1)}, u32[]{:S(2)}) copy-start(bf16[1,512,1024]{2,1,0:T(8,128)(2,1)} %param.13) | copy-start | bytes 3145732
  187.2 1.7 copy-start.3
  189.9 42.7 %all-to-all-start.2 = ((bf16[64,1,8,1024]{3,2,1,0:T(8,128)(2,1)}), bf16[64,1,8,1024]{3,2,1,0:T(8,128)(2,1)S(1)}, u32[]{:S(2)}, u32[]{:S(2)}) async-start(bf16[64,1,8,1024]{3,2,1,0:T(8,128)(2,1)} %split.8), calls=%async_computation.2 | async-start | bytes 2097152 | tf_op jit(solution)/shard_map/all_to_all | solution.py:42
  206.9 34.7 %copy-start.5 = (f32[512,2]{0,1:T(2,128)S(1)}, f32[512,2]{0,1:T(2,128)}, u32[]{:S(2)}) copy-start(f32[512,2]{0,1:T(2,128)} %param.10) | copy-start | bytes 12292
  232.6 1.0 copy-start.2
  233.6 59.1 %all-to-all-start.3 = ((bf16[64,1,16,1024]{3,2,1,0:T(8,128)(2,1)}), bf16[64,1,16,1024]{3,2,1,0:T(8,128)(2,1)S(1)}, u32[]{:S(2)}, u32[]{:S(2)}) async-start(bf16[64,1,16,1024]{3,2,1,0:T(8,128)(2,1)} %split.9), calls=%async_computation.3 | async-start | bytes 4194304 | tf_op jit(solution)/shard_map/all_to_all | solution.py:42
Sparse Core Ops, SparseCore 0:
  137.3 32.3 all-gather.1
where the time goes:
time: 323 us
  waiting for transfers between devices  109 us (34%)
  blocking collectives  99.9 us (31%)
  other arithmetic  36.6 us (11%)
  local copies, waits for them, and re-layouts  35.8 us (11%)
  starting transfers between devices  21.6 us (7%)
  between operations  13.7 us (4%)
  matrix products  5.79 us (2%)
    all_to_all x1, blocking collectives, on_device(): lax.all_to_all(send, 'ep', split_axis=0, concat_axis=0, tiled=True)  94.8 us
    all_to_all x2, waiting for transfers between devices, cut_exchange(): lax.all_to_all(section, axis, split_axis=0, concat_axis=0, tiled=True)  76.8 us
    all_gather x1, waiting for transfers between devices, on_device(): whole_rows = lax.all_gather(received, 'tp', axis=2, tiled=True)  32.5 us
    all_to_all x2, starting transfers between devices, cut_exchange(): lax.all_to_all(section, axis, split_axis=0, concat_axis=0, tiled=True)  21.6 us
    another operation x3, other arithmetic  18.2 us
    scatter x1, local copies, waits for them, and re-layouts, on_device(): jnp.zeros((experts * capacity, half), jnp.bfloat16).at[position]  14.8 us
    reduce_sum x1, other arithmetic, on_device(): jnp.sum(picked.reshape(tok_rows, top, half), axis=1).astype(jnp.bfloat16)  8.58 us
    gather x1, local copies, waits for them, and re-layouts, on_device(): back.reshape(experts * capacity, half)[position].astype(jnp.float32)  7.27 us
  transfers between devices with their start and end apart: 3, of which 3 were waited for; matrix products, arithmetic and copies ran while one was open for 1% of the time, Pallas kernels for 0%

commit v1 on v0

v1 whole, which is shorter than its diff:
```python
import jax
import jax.numpy as jnp
from jax import lax
from jax.experimental import pallas as pl
from jax.experimental.pallas import tpu as pltpu
from jax.sharding import PartitionSpec as P

CHUNKS = ((0, 24),)
BF16 = jnp.bfloat16
F32 = jnp.float32


def block_of(total, most):
    size = most
    while total % size:
        size -= 8
    return size


def strictly_before(n, rows_earlier):
    row = lax.broadcasted_iota(jnp.int32, (n, n), 0)
    col = lax.broadcasted_iota(jnp.int32, (n, n), 1)
    earlier = row < col if rows_earlier else col < row
    return jnp.where(earlier, 1.0, 0.0).astype(BF16)


def select_rows(ids_t, tokens, experts, first, count):
    tok, half = tokens.shape
    per = block_of(experts, 16)

    def kernel(ids_ref, tok_ref, out_ref, key_ref):
        step = pl.program_id(0)

        @pl.when(step == 0)
        def _():
            expert = lax.broadcasted_iota(jnp.int32, (experts, tok), 0)
            named = (ids_ref[0:1, :] == expert) | (ids_ref[1:2, :] == expert)
            named_f = jnp.where(named, 1.0, 0.0)
            slot = jnp.dot(named_f.astype(BF16), strictly_before(tok, True), preferred_element_type=F32)
            key_ref[...] = jnp.where(named, slot, -1.0)

        key = key_ref[pl.ds(pl.multiple_of(step * per, per), per), :]
        wanted = (lax.broadcasted_iota(jnp.int32, (per, count, tok), 1) + first).astype(F32)
        chosen = jnp.where(key[:, None, :] == wanted, 1.0, 0.0).reshape(per * count, tok).astype(BF16)
        out_ref[...] = jnp.dot(chosen, tok_ref[...], preferred_element_type=F32).astype(BF16)

    return pl.pallas_call(
        kernel,
        grid=(experts // per,),
        in_specs=[
            pl.BlockSpec((2, tok), lambda i: (0, 0)),
            pl.BlockSpec((tok, half), lambda i: (0, 0)),
        ],
        out_specs=pl.BlockSpec((per * count, half), lambda i: (i, 0)),
        out_shape=jax.ShapeDtypeStruct((experts * count, half), BF16),
        scratch_shapes=[pltpu.VMEM((experts, tok), F32)],
        cost_estimate=pl.CostEstimate(
            flops=2 * experts * count * tok * half, bytes_accessed=2 * (tok + experts * count) * half, transcendentals=0
        ),
        name="select_rows",
    )(ids_t, tokens)


def hidden_units(core, own, other, gain, w_gate, w_up):
    rows, half = own.shape
    units = w_gate.shape[1]
    block = block_of(rows, 256)

    def kernel(core_ref, own_ref, other_ref, gain_a, gain_b, wg_a, wg_b, wu_a, wu_b, out_ref):
        a = own_ref[...].astype(F32)
        b = other_ref[...].astype(F32)
        total = jnp.sum(a * a, axis=-1, keepdims=True) + jnp.sum(b * b, axis=-1, keepdims=True)
        scale = lax.rsqrt(total * (1.0 / (2 * half)) + 1e-06)
        na = (a * scale * gain_a[0]).astype(BF16)
        nb = (b * scale * gain_b[0]).astype(BF16)
        gate = jnp.dot(na, wg_a[0], preferred_element_type=F32) + jnp.dot(nb, wg_b[0], preferred_element_type=F32)
        upper = jnp.dot(na, wu_a[0], preferred_element_type=F32) + jnp.dot(nb, wu_b[0], preferred_element_type=F32)
        out_ref[...] = (gate / (1.0 + jnp.exp(-gate)) * upper).astype(BF16)

    mine = lambda i, c: (c[0], 0, 0)
    theirs = lambda i, c: (1 - c[0], 0, 0)
    w_gate = w_gate.reshape(2, half, units)
    w_up = w_up.reshape(2, half, units)
    gain = gain.reshape(2, 1, half)
    return pl.pallas_call(
        kernel,
        grid_spec=pltpu.PrefetchScalarGridSpec(
            num_scalar_prefetch=1,
            grid=(rows // block,),
            in_specs=[
                pl.BlockSpec((block, half), lambda i, c: (i, 0)),
                pl.BlockSpec((block, half), lambda i, c: (i, 0)),
                pl.BlockSpec((1, 1, half), mine),
                pl.BlockSpec((1, 1, half), theirs),
                pl.BlockSpec((1, half, units), mine),
                pl.BlockSpec((1, half, units), theirs),
                pl.BlockSpec((1, half, units), mine),
                pl.BlockSpec((1, half, units), theirs),
            ],
            out_specs=pl.BlockSpec((block, units), lambda i, c: (i, 0)),
        ),
        out_shape=jax.ShapeDtypeStruct((rows, units), BF16),
        cost_estimate=pl.CostEstimate(
            flops=8 * rows * half * units, bytes_accessed=4 * rows * half, transcendentals=rows * units
        ),
        name="hidden_units",
    )(core, own, other, gain, gain, w_gate, w_gate, w_up, w_up)


def down_rows(core, own, other, w_down):
    rows, units = own.shape
    half = w_down.shape[1]
    block = block_of(rows, 256)

    def kernel(core_ref, own_ref, other_ref, w_a, w_b, out_ref):
        out = jnp.dot(own_ref[...], w_a[0], preferred_element_type=F32)
        out = out + jnp.dot(other_ref[...], w_b[0], preferred_element_type=F32)
        out_ref[...] = out.astype(BF16)

    w_down = w_down.reshape(2, units, half)
    return pl.pallas_call(
        kernel,
        grid_spec=pltpu.PrefetchScalarGridSpec(
            num_scalar_prefetch=1,
            grid=(rows // block,),
            in_specs=[
                pl.BlockSpec((block, units), lambda i, c: (i, 0)),
                pl.BlockSpec((block, units), lambda i, c: (i, 0)),
                pl.BlockSpec((1, units, half), lambda i, c: (c[0], 0, 0)),
                pl.BlockSpec((1, units, half), lambda i, c: (1 - c[0], 0, 0)),
            ],
            out_specs=pl.BlockSpec((block, half), lambda i, c: (i, 0)),
        ),
        out_shape=jax.ShapeDtypeStruct((rows, half), BF16),
        cost_estimate=pl.CostEstimate(
            flops=4 * rows * half * units, bytes_accessed=2 * rows * (half + 2 * units), transcendentals=0
        ),
        name="down_rows",
    )(core, own, other, w_down, w_down)


def combine(ids, route, back, experts, first, count, before, last):
    tok = ids.shape[0]
    rows, half = back.shape
    block = block_of(rows, 512)
    steps = rows // block

    def kernel(ids_ref, route_ref, back_ref, *rest):
        before_ref = rest[0] if before is not None else None
        out_ref, place_ref, acc_ref = rest[-3:]
        step = pl.program_id(0)

        @pl.when(step == 0)
        def _():
            expert = lax.broadcasted_iota(jnp.int32, (tok, experts), 1)
            one = [ids_ref[:, k : k + 1] == expert for k in range(2)]
            named = jnp.where(one[0] | one[1], 1.0, 0.0).astype(BF16)
            slots = jnp.dot(strictly_before(tok, False), named, preferred_element_type=F32)
            for k in range(2):
                slot = jnp.sum(jnp.where(one[k], slots, 0.0), axis=1, keepdims=True).astype(jnp.int32) - first
                place = ids_ref[:, k : k + 1] * count + slot
                place = jnp.where((slot >= 0) & (slot < count), place, -1)
                place_ref[k] = jnp.broadcast_to(place, (tok, 128))
            if before is None:
                acc_ref[...] = jnp.zeros_like(acc_ref)
            else:
                acc_ref[...] = before_ref[...]

        lane = lax.broadcasted_iota(jnp.int32, (tok, block), 1) + step * block
        weight = jnp.where(place_ref[0, :, 0:1] == lane, route_ref[:, 0:1], 0.0)
        weight = jnp.where(place_ref[1, :, 0:1] == lane, route_ref[:, 1:2], weight)
        acc_ref[...] += jnp.dot(weight.astype(BF16), back_ref[...], preferred_element_type=F32)

        @pl.when(step == steps - 1)
        def _():
            out_ref[...] = acc_ref[...].astype(out_ref.dtype)

    whole = lambda i: (0, 0)
    operands = [ids, route, back]
    in_specs = [
        pl.BlockSpec((tok, 2), whole),
        pl.BlockSpec((tok, 2), whole),
        pl.BlockSpec((block, half), lambda i: (i, 0)),
    ]
    if before is not None:
        operands.append(before)
        in_specs.append(pl.BlockSpec((tok, half), whole))
    return pl.pallas_call(
        kernel,
        grid=(steps,),
        in_specs=in_specs,
        out_specs=pl.BlockSpec((tok, half), whole),
        out_shape=jax.ShapeDtypeStruct((tok, half), BF16 if last else F32),
        scratch_shapes=[pltpu.VMEM((2, tok, 128), jnp.int32), pltpu.VMEM((tok, half), F32)],
        cost_estimate=pl.CostEstimate(
            flops=2 * tok * rows * half, bytes_accessed=2 * (rows + tok) * half, transcendentals=0
        ),
        name="combine",
    )(*operands)


def on_device(tokens, norm_gain, expert_ids, route_weights, gate_weight, up_weight, down_weight):
    half = tokens.shape[1]
    experts = lax.axis_size("ep")
    core = lax.axis_index("tp").astype(jnp.int32).reshape(1)
    swap = [(0, 1), (1, 0)]
    ids_t = expert_ids.T
    w_gate, w_up, w_down = gate_weight[0], up_weight[0], down_weight[0]

    def exchange(array, count):
        array = array.reshape(experts, count, half)
        array = lax.all_to_all(array, "ep", split_axis=0, concat_axis=0, tiled=True)
        return array.reshape(experts * count, half)

    arrived = [
        exchange(select_rows(ids_t, tokens, experts, first, count), count) for first, count in CHUNKS
    ]
    returned = []
    for own, (first, count) in zip(arrived, CHUNKS):
        other = lax.ppermute(own, "tp", swap)
        hidden = hidden_units(core, own, other, norm_gain, w_gate, w_up)
        result = down_rows(core, hidden, lax.ppermute(hidden, "tp", swap), w_down)
        returned.append(exchange(result, count))
    total = None
    for n, (back, (first, count)) in enumerate(zip(returned, CHUNKS)):
        total = combine(expert_ids, route_weights, back, experts, first, count, total, n == len(CHUNKS) - 1)
    return total


def solution(mesh):
    in_specs = (
        P(("grp", "ep"), "tp"),
        P(),
        P(("grp", "ep"), None),
        P(("grp", "ep"), None),
        P("ep", None, "tp"),
        P("ep", None, "tp"),
        P("ep", None, "tp"),
    )
    out_specs = P(("grp", "ep"), "tp")
    return jax.shard_map(
        on_device, mesh=mesh, in_specs=in_specs, out_specs=out_specs, check_vma=False
    )
```

time: 323 us -> 234 us (0.72)
  the two profiles are of different devices: /device:TPU:514 before, /device:TPU:646 now
where the time goes in v1:
time: 234 us; the launch traced here: 232 us
  blocking collectives  96.1 us (41%)
  waiting for transfers between devices  95.8 us (41%)
  Pallas kernels  26.9 us (11%)
  starting transfers between devices  9.28 us (4%)
  local copies, waits for them, and re-layouts  4.27 us (2%)
    all_to_all x1, blocking collectives, exchange(): array = lax.all_to_all(array, 'ep', split_axis=0, concat_axis=0, tiled=True)  96.1 us
    all_to_all x1, waiting for transfers between devices, exchange(): array = lax.all_to_all(array, 'ep', split_axis=0, concat_axis=0, tiled=True)  87.6 us
    all_to_all x1, starting transfers between devices, exchange(): array = lax.all_to_all(array, 'ep', split_axis=0, concat_axis=0, tiled=True)  9.17 us
    pallas_call x1, Pallas kernels, hidden_units(): pl.pallas_call(kernel, grid_spec=pltpu.PrefetchScalarGridSpec(num_scalar_...  9.03 us
    pallas_call x1, Pallas kernels, down_rows(): pl.pallas_call(kernel, grid_spec=pltpu.PrefetchScalarGridSpec(num_scalar_...  6.45 us
    pallas_call x1, Pallas kernels, combine(): pl.pallas_call(kernel, grid=(steps,), in_specs=in_specs, out_specs=pl.Blo...  6.41 us
    ppermute x1, waiting for transfers between devices, on_device(): other = lax.ppermute(own, 'tp', swap)  5.79 us
    pallas_call x1, Pallas kernels, select_rows(): pl.pallas_call(kernel, grid=(experts // per,), in_specs=[pl.BlockSpec((2,...  4.97 us
  transfers between devices with their start and end apart: 3, of which 3 were waited for; matrix products, arithmetic and copies ran while one was open for 1% of the time, Pallas kernels for 0%

profile of v1, /device:TPU:646, one launch (start us, length us, event | category | flops | bytes accessed | tf_op | source)
XLA Modules:
  0.0 232.4 jit_solution(5646272609609392612)
XLA Ops:
  0.0 5.0 %select_rows.1 = bf16[1536,1024]{1,0:T(8,128)(2,1)} custom-call(s32[2,512]{1,0:T(2,128)} %bitcast.17, bf16[512,1024]{1,0:T(8,128)(2,1)} %tok_ref.1), custom_call_target="tpu_custom_call" | custom-call | flops 1610612736 | bytes 4194304 | tf_op jit(solution)/shard_map/select_rows/pallas_call | solution.py:47
  5.0 96.1 %all_to_all.10 = bf16[64,24,1024]{2,1,0:T(8,128)(2,1)S(1)} all-to-all(bf16[64,24,1024]{2,1,0:T(8,128)(2,1)} %bitcast.16), channel_id=1, replica_groups=mesh['grp'=2,'ep'=64,'tp'=2] {'ep'}, dimensions={0} | all-to-all | bytes 6291456 | tf_op jit(solution)/shard_map/all_to_all | solution.py:212
  101.1 0.0 copy-start
  101.1 0.0 collective-permute-start
  101.1 5.8 %collective-permute-done.other_ref = bf16[1536,1024]{1,0:T(8,128)(2,1)} collective-permute-done((bf16[1536,1024]{1,0:T(8,128)(2,1)S(1)}, bf16[1536,1024]{1,0:T(8,128)(2,1)}, u32[]{:S(2)}, u32[]{:S(2)}) %collective-permute-start) | collective-permute-done | bytes 3145760 | tf_op jit(solution)/shard_map/ppermute | solution.py:220
  106.9 0.0 copy-done
  106.9 9.0 %hidden_units.1.own_ref = bf16[1536,256]{1,0:T(8,128)(2,1)} custom-call(s32[1]{0:T(128)} %bitcast.core_ref, bf16[1536,1024]{1,0:T(8,128)(2,1)} %bitcast.14, bf16[1536,1024]{1,0:T(8,128)(2,1)} %collective-permute-done.other_ref, f32[2,1,1024]{2,1,0:T(1,128)} %bitcast.22, f32[2,1,1024]{2,1,0:T(1,128)} %bitcast.23, bf16[2,1024,256]{2,1,0:T(8,128)(2,1)} %bitcast.18, ...), custom_call_target="tpu_custom_call" | custom-call | flops 3221225472 | bytes 6291456 | tf_op jit(solution)/shard_map/hidden_units/pallas_call | solution.py:85
  115.9 0.1 collective-permute-start.1
  116.0 2.4 %collective-permute-done.1.other_ref = bf16[1536,256]{1,0:T(8,128)(2,1)S(1)} collective-permute-done((bf16[1536,256]{1,0:T(8,128)(2,1)}, bf16[1536,256]{1,0:T(8,128)(2,1)S(1)}, u32[]{:S(2)}, u32[]{:S(2)}) %collective-permute-start.1) | collective-permute-done | bytes 786464 | tf_op jit(solution)/shard_map/ppermute | solution.py:222
  118.4 0.0 copy-start.2
  118.4 0.9 copy-done.2
  119.3 6.5 %down_rows.1 = bf16[1536,1024]{1,0:T(8,128)(2,1)} custom-call(s32[1]{0:T(128)} %bitcast.core_ref, bf16[1536,256]{1,0:T(8,128)(2,1)} %hidden_units.1.own_ref, bf16[1536,256]{1,0:T(8,128)(2,1)} %copy-done.2, bf16[2,256,1024]{2,1,0:T(8,128)(2,1)} %bitcast.11, bf16[2,256,1024]{2,1,0:T(8,128)(2,1)} %bitcast.12), custom_call_target="tpu_custom_call" | custom-call | flops 1610612736 | bytes 4718592 | tf_op jit(solution)/shard_map/down_rows/pallas_call | solution.py:121
  125.7 0.0 copy-start.3
  125.7 0.0 copy-start.4
  125.8 9.2 %all-to-all-start.1 = ((bf16[64,24,1024]{2,1,0:T(8,128)(2,1)}), bf16[64,24,1024]{2,1,0:T(8,128)(2,1)S(1)}, u32[]{:S(2)}, u32[]{:S(2)}) async-start(bf16[64,24,1024]{2,1,0:T(8,128)(2,1)} %bitcast.10), calls=%async_computation.1 | async-start | bytes 6291456 | tf_op jit(solution)/shard_map/all_to_all | solution.py:212
  134.9 0.0 copy-done.3
  134.9 0.9 copy.8.ids_ref
  135.8 0.0 copy-done.4
  135.8 0.9 copy.9.route_ref
  136.7 87.6 %all-to-all-done.1 = bf16[64,24,1024]{2,1,0:T(8,128)(2,1)S(1)} async-done(((bf16[64,24,1024]{2,1,0:T(8,128)(2,1)}), bf16[64,24,1024]{2,1,0:T(8,128)(2,1)S(1)}, u32[]{:S(2)}, u32[]{:S(2)}) %all-to-all-start.1) | async-done | bytes 3145760 | tf_op jit(solution)/shard_map/all_to_all | solution.py:212
  224.3 0.0 copy-start.1
  224.3 1.6 copy-done.1
  225.9 6.4 %combine.1 = bf16[512,1024]{1,0:T(8,128)(2,1)} custom-call(s32[512,2]{1,0:T(8,128)} %copy.8.ids_ref, f32[512,2]{1,0:T(8,128)} %copy.9.route_ref, bf16[1536,1024]{1,0:T(8,128)(2,1)} %bitcast.15), custom_call_target="tpu_custom_call" | custom-call | flops 1610612736 | bytes 4194304 | tf_op jit(solution)/shard_map/combine/pallas_call | solution.py:188
Async XLA Ops:
  101.1 5.8 %copy-start = (bf16[64,24,1024]{2,1,0:T(8,128)(2,1)}, bf16[64,24,1024]{2,1,0:T(8,128)(2,1)S(1)}, u32[]{:S(2)}) copy-start(bf16[64,24,1024]{2,1,0:T(8,128)(2,1)S(1)} %all_to_all.10) | copy-start | bytes 9437188
  101.1 5.8 %collective-permute-start = (bf16[1536,1024]{1,0:T(8,128)(2,1)S(1)}, bf16[1536,1024]{1,0:T(8,128)(2,1)}, u32[]{:S(2)}, u32[]{:S(2)}) collective-permute-start(bf16[1536,1024]{1,0:T(8,128)(2,1)S(1)} %bitcast.13), channel_id=1, source_target_pairs={{0,1},{1,0},{2,3},{3,2},{4,5},{5,4},{6,7},{7,6},{8,9},{9,8},{10,11... | collective-permute-start | bytes 9437192 | tf_op jit(solution)/shard_map/ppermute | solution.py:220
  115.9 2.5 %collective-permute-start.1 = (bf16[1536,256]{1,0:T(8,128)(2,1)}, bf16[1536,256]{1,0:T(8,128)(2,1)S(1)}, u32[]{:S(2)}, u32[]{:S(2)}) collective-permute-start(bf16[1536,256]{1,0:T(8,128)(2,1)} %hidden_units.1.own_ref), channel_id=1, source_target_pairs={{0,1},{1,0},{2,3},{3,2},{4,5},{5,4},{6,7},{7,6},{8,9},{9,8},{10,11... | collective-permute-start | bytes 2359304 | tf_op jit(solution)/shard_map/ppermute | solution.py:222
  118.4 0.9 copy-start.2
  125.7 9.2 %copy-start.3 = (s32[512,2]{0,1:T(2,128)S(1)}, s32[512,2]{0,1:T(2,128)}, u32[]{:S(2)}) copy-start(s32[512,2]{0,1:T(2,128)} %param.9) | copy-start | bytes 12292
  125.7 10.1 %copy-start.4 = (f32[512,2]{0,1:T(2,128)S(1)}, f32[512,2]{0,1:T(2,128)}, u32[]{:S(2)}) copy-start(f32[512,2]{0,1:T(2,128)} %param.10) | copy-start | bytes 12292
  125.8 98.5 %all-to-all-start.1 = ((bf16[64,24,1024]{2,1,0:T(8,128)(2,1)}), bf16[64,24,1024]{2,1,0:T(8,128)(2,1)S(1)}, u32[]{:S(2)}, u32[]{:S(2)}) async-start(bf16[64,24,1024]{2,1,0:T(8,128)(2,1)} %bitcast.10), calls=%async_computation.1 | async-start | bytes 6291456 | tf_op jit(solution)/shard_map/all_to_all | solution.py:212
  224.3 1.6 copy-start.1

commit v2 on v1

v2 whole, which is shorter than its diff:
```python
import jax
import jax.numpy as jnp
from jax import lax
from jax.experimental import pallas as pl
from jax.experimental.pallas import tpu as pltpu
from jax.sharding import PartitionSpec as P

CAPACITY = 24
PIECES = 3
VMEM = 20 * 1024 * 1024
BF16 = jnp.bfloat16
F32 = jnp.float32
ANY = pl.BlockSpec(memory_space=pl.ANY)


def block_of(total, most):
    size = most
    while total % size:
        size -= 8
    return size


def slots_of(ids_ref, experts):
    tok = ids_ref.shape[1]
    expert = lax.broadcasted_iota(jnp.int32, (experts, tok), 0)
    one = [ids_ref[k : k + 1, :] == expert for k in range(2)]
    named = one[0] | one[1]
    row = lax.broadcasted_iota(jnp.int32, (tok, tok), 0)
    col = lax.broadcasted_iota(jnp.int32, (tok, tok), 1)
    before = jnp.where(row < col, 1.0, 0.0).astype(BF16)
    slot = jnp.dot(jnp.where(named, 1.0, 0.0).astype(BF16), before, preferred_element_type=F32)
    return one, named, slot


def select_rows(ids_t, tokens, experts):
    tok, half = tokens.shape
    per = block_of(experts, 16)

    def kernel(ids_ref, tok_ref, out_ref, key_ref):
        step = pl.program_id(0)

        @pl.when(step == 0)
        def _():
            _, named, slot = slots_of(ids_ref, experts)
            key_ref[...] = jnp.where(named, slot, -1.0)

        key = key_ref[pl.ds(pl.multiple_of(step * per, per), per), :]
        wanted = lax.broadcasted_iota(jnp.int32, (per, CAPACITY, tok), 1).astype(F32)
        chosen = jnp.where(key[:, None, :] == wanted, 1.0, 0.0).reshape(per * CAPACITY, tok).astype(BF16)
        out_ref[...] = jnp.dot(chosen, tok_ref[...], preferred_element_type=F32).astype(BF16)

    return pl.pallas_call(
        kernel,
        grid=(experts // per,),
        in_specs=[
            pl.BlockSpec((2, tok), lambda i: (0, 0)),
            pl.BlockSpec((tok, half), lambda i: (0, 0)),
        ],
        out_specs=pl.BlockSpec((per * CAPACITY, half), lambda i: (i, 0)),
        out_shape=jax.ShapeDtypeStruct((experts * CAPACITY, half), BF16),
        scratch_shapes=[pltpu.VMEM((experts, tok), F32)],
        cost_estimate=pl.CostEstimate(
            flops=2 * experts * CAPACITY * tok * half,
            bytes_accessed=2 * (tok + experts * CAPACITY) * half,
            transcendentals=0,
        ),
        compiler_params=pltpu.CompilerParams(vmem_limit_bytes=VMEM),
        name="select_rows",
    )(ids_t, tokens)


def combine_matrix(ids_t, route_t, experts, after):
    tok = ids_t.shape[1]
    rows = experts * CAPACITY

    def kernel(ids_ref, route_ref, after_ref, out_ref):
        one, _, slot = slots_of(ids_ref, experts)
        places = []
        for k in range(2):
            mine = jnp.sum(jnp.where(one[k], slot, 0.0), axis=0, keepdims=True)
            places.append(ids_ref[k : k + 1, :].astype(F32) * CAPACITY + mine)
        lines = jnp.concatenate(places + [route_ref[...], jnp.zeros((4, tok), F32)], axis=0).T
        lane = lax.broadcasted_iota(jnp.int32, (tok, rows), 1).astype(F32)
        weight = jnp.where(lines[:, 0:1] == lane, lines[:, 2:3], 0.0)
        out_ref[...] = jnp.where(lines[:, 1:2] == lane, lines[:, 3:4], weight).astype(BF16)

    return pl.pallas_call(
        kernel,
        in_specs=[
            pl.BlockSpec((2, tok), lambda: (0, 0)),
            pl.BlockSpec((2, tok), lambda: (0, 0)),
            ANY,
        ],
        out_specs=pl.BlockSpec((tok, rows), lambda: (0, 0)),
        out_shape=jax.ShapeDtypeStruct((tok, rows), BF16),
        cost_estimate=pl.CostEstimate(flops=4 * tok * rows, bytes_accessed=2 * tok * rows, transcendentals=0),
        compiler_params=pltpu.CompilerParams(vmem_limit_bytes=VMEM),
        name="combine_matrix",
    )(ids_t, route_t, after)


def hidden_units(core, own, other, first, gain, w_gate, w_up):
    rows, half = other.shape
    units = w_gate.shape[1]
    block = block_of(rows, 256)
    skip = first // block

    def kernel(core_ref, own_ref, other_ref, gain_a, gain_b, wg_a, wg_b, wu_a, wu_b, out_ref):
        a = own_ref[...].astype(F32)
        b = other_ref[...].astype(F32)
        total = jnp.sum(a * a, axis=-1, keepdims=True) + jnp.sum(b * b, axis=-1, keepdims=True)
        scale = lax.rsqrt(total * (1.0 / (2 * half)) + 1e-06)
        na = (a * scale * gain_a[0]).astype(BF16)
        nb = (b * scale * gain_b[0]).astype(BF16)
        gate = jnp.dot(na, wg_a[0], preferred_element_type=F32) + jnp.dot(nb, wg_b[0], preferred_element_type=F32)
        upper = jnp.dot(na, wu_a[0], preferred_element_type=F32) + jnp.dot(nb, wu_b[0], preferred_element_type=F32)
        out_ref[...] = (gate / (1.0 + jnp.exp(-gate)) * upper).astype(BF16)

    mine = lambda i, c: (c[0], 0, 0)
    theirs = lambda i, c: (1 - c[0], 0, 0)
    w_gate = w_gate.reshape(2, half, units)
    w_up = w_up.reshape(2, half, units)
    gain = gain.reshape(2, 1, half)
    return pl.pallas_call(
        kernel,
        grid_spec=pltpu.PrefetchScalarGridSpec(
            num_scalar_prefetch=1,
            grid=(rows // block,),
            in_specs=[
                pl.BlockSpec((block, half), lambda i, c: (i + skip, 0)),
                pl.BlockSpec((block, half), lambda i, c: (i, 0)),
                pl.BlockSpec((1, 1, half), mine),
                pl.BlockSpec((1, 1, half), theirs),
                pl.BlockSpec((1, half, units), mine),
                pl.BlockSpec((1, half, units), theirs),
                pl.BlockSpec((1, half, units), mine),
                pl.BlockSpec((1, half, units), theirs),
            ],
            out_specs=pl.BlockSpec((block, units), lambda i, c: (i, 0)),
        ),
        out_shape=jax.ShapeDtypeStruct((rows, units), BF16),
        cost_estimate=pl.CostEstimate(
            flops=8 * rows * half * units, bytes_accessed=4 * rows * half, transcendentals=rows * units
        ),
        compiler_params=pltpu.CompilerParams(vmem_limit_bytes=VMEM),
        name="hidden_units",
    )(core, own, other, gain, gain, w_gate, w_gate, w_up, w_up)


def down_rows(core, own, other, first, w_down, total, result, after):
    rows, units = own.shape
    half = w_down.shape[1]
    block = block_of(rows, 256)
    skip = first // block

    def kernel(core_ref, own_ref, other_ref, w_a, w_b, *rest):
        out = jnp.dot(own_ref[...], w_a[0], preferred_element_type=F32)
        out = out + jnp.dot(other_ref[...], w_b[0], preferred_element_type=F32)
        rest[-1][...] = out.astype(BF16)

    w_down = w_down.reshape(2, units, half)
    operands = [core, own, other, w_down, w_down]
    in_specs = [
        pl.BlockSpec((block, units), lambda i, c: (i, 0)),
        pl.BlockSpec((block, units), lambda i, c: (i, 0)),
        pl.BlockSpec((1, units, half), lambda i, c: (c[0], 0, 0)),
        pl.BlockSpec((1, units, half), lambda i, c: (1 - c[0], 0, 0)),
    ]
    aliases = {}
    if after is not None:
        operands.append(after)
        in_specs.append(ANY)
    if result is not None:
        aliases = {len(operands): 0}
        operands.append(result)
        in_specs.append(ANY)
    return pl.pallas_call(
        kernel,
        grid_spec=pltpu.PrefetchScalarGridSpec(
            num_scalar_prefetch=1,
            grid=(rows // block,),
            in_specs=in_specs,
            out_specs=pl.BlockSpec((block, half), lambda i, c: (i + skip, 0)),
        ),
        out_shape=jax.ShapeDtypeStruct((total, half), BF16),
        input_output_aliases=aliases,
        cost_estimate=pl.CostEstimate(
            flops=4 * rows * half * units, bytes_accessed=2 * rows * (half + 2 * units), transcendentals=0
        ),
        compiler_params=pltpu.CompilerParams(vmem_limit_bytes=VMEM),
        name="down_rows",
    )(*operands)


def combine(weights, back):
    tok, rows = weights.shape
    half = back.shape[1]
    block = 256

    def kernel(weights_ref, back_ref, out_ref):
        out_ref[...] = jnp.dot(weights_ref[...], back_ref[...], preferred_element_type=F32).astype(BF16)

    return pl.pallas_call(
        kernel,
        grid=(half // block,),
        in_specs=[
            pl.BlockSpec((tok, rows), lambda i: (0, 0)),
            pl.BlockSpec((rows, block), lambda i: (0, i)),
        ],
        out_specs=pl.BlockSpec((tok, block), lambda i: (0, i)),
        out_shape=jax.ShapeDtypeStruct((tok, half), BF16),
        cost_estimate=pl.CostEstimate(
            flops=2 * tok * rows * half, bytes_accessed=2 * (rows * (half + tok) + tok * half), transcendentals=0
        ),
        compiler_params=pltpu.CompilerParams(vmem_limit_bytes=VMEM),
        name="combine",
    )(weights, back)


def on_device(tokens, norm_gain, expert_ids, route_weights, gate_weight, up_weight, down_weight):
    half = tokens.shape[1]
    experts = lax.axis_size("ep")
    core = lax.axis_index("tp").astype(jnp.int32).reshape(1)
    swap = [(0, 1), (1, 0)]
    ids_t, route_t = expert_ids.T, route_weights.T
    w_gate, w_up, w_down = gate_weight[0], up_weight[0], down_weight[0]
    rows = experts * CAPACITY

    def exchange(array):
        array = array.reshape(experts, CAPACITY, half)
        array = lax.all_to_all(array, "ep", split_axis=0, concat_axis=0, tiled=True)
        return array.reshape(rows, half)

    own = exchange(select_rows(ids_t, tokens, experts))
    length = rows // PIECES
    starts = range(0, rows, length)
    others = [lax.ppermute(own[first : first + length], "tp", swap) for first in starts]
    weights = combine_matrix(ids_t, route_t, experts, own)
    hidden = [
        hidden_units(core, own, other, first, norm_gain, w_gate, w_up) for first, other in zip(starts, others)
    ]
    crossed = [lax.ppermute(piece, "tp", swap) for piece in hidden]
    result = None
    for first, mine, theirs in zip(starts, hidden, crossed):
        after = weights if result is None else None
        result = down_rows(core, mine, theirs, first, w_down, rows, result, after)
    return combine(weights, exchange(result))


def solution(mesh):
    in_specs = (
        P(("grp", "ep"), "tp"),
        P(),
        P(("grp", "ep"), None),
        P(("grp", "ep"), None),
        P("ep", None, "tp"),
        P("ep", None, "tp"),
        P("ep", None, "tp"),
    )
    out_specs = P(("grp", "ep"), "tp")
    return jax.shard_map(
        on_device, mesh=mesh, in_specs=in_specs, out_specs=out_specs, check_vma=False
    )
```

time: 234 us -> 210 us (0.90)
  waiting for transfers between devices: 95.8 us -> 2.5 us
  blocking collectives: 96.1 us -> 180 us
  Pallas kernels: 26.9 us -> 18.8 us
  starting transfers between devices: 9.28 us -> 1.53 us
    all_to_all x1 -> x0, waiting for transfers between devices: 87.6 us -> none  [exchange(): array = lax.all_to_all(array, 'ep', split_axis=0, concat_axis=0, tiled=True)]
    all_to_all x1 -> x2, blocking collectives: 96.1 us -> 180 us  [exchange(): array = lax.all_to_all(array, 'ep', split_axis=0, concat_axis=0, tiled=True)]
    all_to_all x1 -> x0, starting transfers between devices: 9.17 us -> none  [exchange(): array = lax.all_to_all(array, 'ep', split_axis=0, concat_axis=0, tiled=True)]
    ppermute x2 -> x6, waiting for transfers between devices: 8.18 us -> 2.5 us  [the longest x3 2.49 us: on_device(): lax.ppermute(own[first:first + length], 'tp', swap)]
    pallas_call x1 -> x3, Pallas kernels: 6.45 us -> 2.77 us  [down_rows(): pl.pallas_call(kernel, grid_spec=pltpu.PrefetchScalarGridSpec(num_scalar_...]
    pallas_call x1, Pallas kernels: 4.97 us -> 2.55 us  [select_rows(): pl.pallas_call(kernel, grid=(experts // per,), in_specs=[pl.BlockSpec((2,...]
    pallas_call x1 -> x2, Pallas kernels: 6.41 us -> 4.43 us  [the longest x1 3.47 us: combine(): pl.pallas_call(kernel, grid=(half // block,), in_specs=[pl.BlockSpec((tok...]
    pallas_call x1 -> x3, Pallas kernels: 9.03 us -> 9.01 us  [hidden_units(): pl.pallas_call(kernel, grid_spec=pltpu.PrefetchScalarGridSpec(num_scalar_...]
  transfers between devices with their start and end apart: 3 -> 6, of which waited for: 3 -> 1; matrix products, arithmetic and copies ran while one was open for 1% -> 0% of each run, Pallas kernels for 0% -> 6%
where the time goes in v2:
time: 210 us; the launch traced here: 209 us
  blocking collectives  180 us (86%)
  Pallas kernels  18.8 us (9%)
  local copies, waits for them, and re-layouts  6.13 us (3%)
  waiting for transfers between devices  2.5 us (1%)
    all_to_all x2, blocking collectives, exchange(): array = lax.all_to_all(array, 'ep', split_axis=0, concat_axis=0, tiled=True)  180 us
    pallas_call x3, Pallas kernels, hidden_units(): pl.pallas_call(kernel, grid_spec=pltpu.PrefetchScalarGridSpec(num_scalar_...  9.01 us
    unnamed x18, local copies, waits for them, and re-layouts  4.39 us
  transfers between devices with their start and end apart: 6, of which 1 were waited for; matrix products, arithmetic and copies ran while one was open for 0% of the time, Pallas kernels for 6%

profile of v2, /device:TPU:646, one launch (start us, length us, event | category | flops | bytes accessed | tf_op | source)
XLA Modules:
  0.0 209.4 jit_solution(10825153995137254511)
XLA Ops:
  0.0 0.7 copy-done.5
  0.7 1.2 copy-done.8
  1.9 2.5 %select_rows.1 = bf16[1536,1024]{1,0:T(8,128)(2,1)S(1)} custom-call(s32[2,512]{1,0:T(2,128)S(1)} %bitcast.43, bf16[512,1024]{1,0:T(8,128)(2,1)S(1)} %copy-done.8), custom_call_target="tpu_custom_call" | custom-call | flops 1610612736 | bytes 4194304 | tf_op jit(solution)/shard_map/select_rows/pallas_call | solution.py:52
  4.5 95.4 %all_to_all.10 = bf16[64,24,1024]{2,1,0:T(8,128)(2,1)S(1)} all-to-all(bf16[64,24,1024]{2,1,0:T(8,128)(2,1)S(1)} %bitcast.36), channel_id=1, replica_groups=mesh['grp'=2,'ep'=64,'tp'=2] {'ep'}, dimensions={0} | all-to-all | bytes 6291456 | tf_op jit(solution)/shard_map/all_to_all | solution.py:231
  99.9 1.7 fusion
  101.6 0.0 collective-permute-start.4
  101.7 0.5 collective-permute-start.2
  102.2 0.0 collective-permute-start
  102.2 2.5 %collective-permute-done.4.other_ref = bf16[512,1024]{1,0:T(8,128)(2,1)} collective-permute-done((bf16[512,1024]{1,0:T(8,128)(2,1)}, bf16[512,1024]{1,0:T(8,128)(2,1)}, u32[]{:S(2)}, u32[]{:S(2)}) %collective-permute-start.4) | collective-permute-done | bytes 1048608 | tf_op jit(solution)/shard_map/ppermute | solution.py:237
  104.7 1.2 copy-done
  105.9 1.2 copy-done.2
  107.1 3.0 %hidden_units.5.own_ref = bf16[512,256]{1,0:T(8,128)(2,1)S(1)} custom-call(s32[1]{0:T(128)} %bitcast.4.core_ref, bf16[1536,1024]{1,0:T(8,128)(2,1)S(1)} %bitcast.12, bf16[512,1024]{1,0:T(8,128)(2,1)} %collective-permute-done.4.other_ref, f32[2,1,1024]{2,1,0:T(1,128)S(1)} %bitcast.37, f32[2,1,1024]{2,1,0:T(1,128)S(1)} %bitcast.38, ...), custom_call_target="tpu_custom_call" | custom-call | flops 1073741824 | bytes 2097152 | tf_op jit(solution)/shard_map/hidden_units/pallas_call | solution.py:124
  110.1 0.0 copy-start.1
  110.1 0.3 collective-permute-start.5
  110.4 0.0 collective-permute-done.2.other_ref
  110.4 3.0 %hidden_units.4.own_ref = bf16[512,256]{1,0:T(8,128)(2,1)S(1)} custom-call(s32[1]{0:T(128)} %bitcast.4.core_ref, bf16[1536,1024]{1,0:T(8,128)(2,1)S(1)} %bitcast.13, bf16[512,1024]{1,0:T(8,128)(2,1)} %collective-permute-done.2.other_ref, f32[2,1,1024]{2,1,0:T(1,128)S(1)} %bitcast.39, f32[2,1,1024]{2,1,0:T(1,128)S(1)} %bitcast.40, ...), custom_call_target="tpu_custom_call" | custom-call | flops 1073741824 | bytes 2097152 | tf_op jit(solution)/shard_map/hidden_units/pallas_call | solution.py:124
  113.4 0.0 copy-start.6
  113.4 0.0 copy-start.7
  113.5 0.4 collective-permute-start.3
  113.9 0.0 collective-permute-done.other_ref
  113.9 3.0 %hidden_units.3.own_ref = bf16[512,256]{1,0:T(8,128)(2,1)S(1)} custom-call(s32[1]{0:T(128)} %bitcast.4.core_ref, bf16[1536,1024]{1,0:T(8,128)(2,1)S(1)} %bitcast.14, bf16[512,1024]{1,0:T(8,128)(2,1)} %collective-permute-done.other_ref, f32[2,1,1024]{2,1,0:T(1,128)S(1)} %bitcast.41, f32[2,1,1024]{2,1,0:T(1,128)S(1)} %bitcast.42, ...), custom_call_target="tpu_custom_call" | custom-call | flops 1073741824 | bytes 2097152 | tf_op jit(solution)/shard_map/hidden_units/pallas_call | solution.py:124
  116.9 0.0 copy-start.3
  116.9 0.3 collective-permute-start.1
  117.2 1.0 combine_matrix.1.rest_0_.weights_ref
  118.2 0.0 collective-permute-done.5.other_ref
  118.2 0.9 down_rows.3.rest_0_
  119.1 0.0 collective-permute-done.3.other_ref
  119.2 0.9 down_rows.4.rest_0_
  120.1 0.0 collective-permute-done.1.other_ref
  120.1 0.9 down_rows.5
  121.0 84.9 %all_to_all.11 = bf16[64,24,1024]{2,1,0:T(8,128)(2,1)S(1)} all-to-all(bf16[64,24,1024]{2,1,0:T(8,128)(2,1)S(1)} %bitcast.16), channel_id=1, replica_groups=mesh['grp'=2,'ep'=64,'tp'=2] {'ep'}, dimensions={0} | all-to-all | bytes 6291456 | tf_op jit(solution)/shard_map/all_to_all | solution.py:231
  205.9 3.5 %combine.1 = bf16[512,1024]{1,0:T(8,128)(2,1)} custom-call(bf16[512,1536]{1,0:T(8,128)(2,1)S(1)} %combine_matrix.1.rest_0_.weights_ref, bf16[1536,1024]{1,0:T(8,128)(2,1)S(1)} %bitcast.35), custom_call_target="tpu_custom_call" | custom-call | flops 1610612736 | bytes 5767168 | tf_op jit(solution)/shard_map/combine/pallas_call | solution.py:203
  (10 shorter events, 0.0 us)
Async XLA Ops:
  0.0 0.7 copy-start.5
  0.7 1.2 copy-start.8
  99.9 4.7 %copy-start.4 = (f32[2048]{0:T(1024)S(1)}, f32[2048]{0:T(1024)}, u32[]{:S(2)}) copy-start(f32[2048]{0:T(1024)} %param.8) | copy-start | bytes 24580
  101.6 3.0 %collective-permute-start.4 = (bf16[512,1024]{1,0:T(8,128)(2,1)}, bf16[512,1024]{1,0:T(8,128)(2,1)}, u32[]{:S(2)}, u32[]{:S(2)}) collective-permute-start(bf16[512,1024]{1,0:T(8,128)(2,1)} %get-tuple-element.5), channel_id=1, source_target_pairs={{0,1},{1,0},{2,3},{3,2},{4,5},{5,4},{6,7},{7,6},{8,9},{9,8},{10,11... | collective-permute-start | bytes 3145736 | tf_op jit(solution)/shard_map/ppermute | solution.py:237
  101.7 8.7 %collective-permute-start.2 = (bf16[512,1024]{1,0:T(8,128)(2,1)}, bf16[512,1024]{1,0:T(8,128)(2,1)}, u32[]{:S(2)}, u32[]{:S(2)}) collective-permute-start(bf16[512,1024]{1,0:T(8,128)(2,1)} %get-tuple-element.6), channel_id=1, source_target_pairs={{0,1},{1,0},{2,3},{3,2},{4,5},{5,4},{6,7},{7,6},{8,9},{9,8},{10,11... | collective-permute-start | bytes 3145736 | tf_op jit(solution)/shard_map/ppermute | solution.py:237
  102.2 11.7 %collective-permute-start = (bf16[512,1024]{1,0:T(8,128)(2,1)}, bf16[512,1024]{1,0:T(8,128)(2,1)}, u32[]{:S(2)}, u32[]{:S(2)}) collective-permute-start(bf16[512,1024]{1,0:T(8,128)(2,1)} %get-tuple-element.7), channel_id=1, source_target_pairs={{0,1},{1,0},{2,3},{3,2},{4,5},{5,4},{6,7},{7,6},{8,9},{9,8},{10,11... | collective-permute-start | bytes 3145736 | tf_op jit(solution)/shard_map/ppermute | solution.py:237
  104.7 1.2 copy-start
  105.9 1.2 copy-start.2
  110.1 3.8 %copy-start.1 = (bf16[1,2048,256]{2,1,0:T(8,128)(2,1)S(1)}, bf16[1,2048,256]{2,1,0:T(8,128)(2,1)}, u32[]{:S(2)}) copy-start(bf16[1,2048,256]{2,1,0:T(8,128)(2,1)} %param.11) | copy-start | bytes 3145732
  110.1 8.1 %collective-permute-start.5 = (bf16[512,256]{1,0:T(8,128)(2,1)S(1)}, bf16[512,256]{1,0:T(8,128)(2,1)S(1)}, u32[]{:S(2)}, u32[]{:S(2)}) collective-permute-start(bf16[512,256]{1,0:T(8,128)(2,1)S(1)} %hidden_units.5.own_ref), channel_id=1, source_target_pairs={{0,1},{1,0},{2,3},{3,2},{4,5},{5,4},{6,7},{7,6},{8,9},{9,8},{10,11... | collective-permute-start | bytes 786440 | tf_op jit(solution)/shard_map/ppermute | solution.py:242
  113.4 3.8 %copy-start.6 = (s32[512,2]{0,1:T(2,128)S(1)}, s32[512,2]{0,1:T(2,128)}, u32[]{:S(2)}) copy-start(s32[512,2]{0,1:T(2,128)} %param.9) | copy-start | bytes 12292
  113.4 3.8 %copy-start.7 = (f32[512,2]{0,1:T(2,128)S(1)}, f32[512,2]{0,1:T(2,128)}, u32[]{:S(2)}) copy-start(f32[512,2]{0,1:T(2,128)} %param.10) | copy-start | bytes 12292
  113.5 5.7 %collective-permute-start.3 = (bf16[512,256]{1,0:T(8,128)(2,1)S(1)}, bf16[512,256]{1,0:T(8,128)(2,1)S(1)}, u32[]{:S(2)}, u32[]{:S(2)}) collective-permute-start(bf16[512,256]{1,0:T(8,128)(2,1)S(1)} %hidden_units.4.own_ref), channel_id=1, source_target_pairs={{0,1},{1,0},{2,3},{3,2},{4,5},{5,4},{6,7},{7,6},{8,9},{9,8},{10,11... | collective-permute-start | bytes 786440 | tf_op jit(solution)/shard_map/ppermute | solution.py:242
  116.9 1.3 copy-start.3
  116.9 3.2 %collective-permute-start.1 = (bf16[512,256]{1,0:T(8,128)(2,1)S(1)}, bf16[512,256]{1,0:T(8,128)(2,1)S(1)}, u32[]{:S(2)}, u32[]{:S(2)}) collective-permute-start(bf16[512,256]{1,0:T(8,128)(2,1)S(1)} %hidden_units.3.own_ref), channel_id=1, source_target_pairs={{0,1},{1,0},{2,3},{3,2},{4,5},{5,4},{6,7},{7,6},{8,9},{9,8},{10,11... | collective-permute-start | bytes 786440 | tf_op jit(solution)/shard_map/ppermute | solution.py:242

commit v3 on v2

--- a/solution.py
+++ b/solution.py
@@ -7,10 +7,12 @@
 
 CAPACITY = 24
 PIECES = 3
-VMEM = 20 * 1024 * 1024
+PARAMS = pltpu.CompilerParams(vmem_limit_bytes=20 * 1024 * 1024)
 BF16 = jnp.bfloat16
 F32 = jnp.float32
 ANY = pl.BlockSpec(memory_space=pl.ANY)
+SCALAR = pl.BlockSpec(memory_space=pltpu.SMEM)
+ONCHIP = pl.BlockSpec(memory_space=pltpu.VMEM)
 
 
 def block_of(total, most):
@@ -32,11 +34,11 @@
     return one, named, slot
 
 
-def select_rows(ids_t, tokens, experts):
+def select_rows(core, ids_t, tokens, experts):
     tok, half = tokens.shape
     per = block_of(experts, 16)
 
-    def kernel(ids_ref, tok_ref, out_ref, key_ref):
+    def kernel(core_ref, ids_ref, tok_ref, out_ref, key_ref):
         step = pl.program_id(0)
 
         @pl.when(step == 0)
@@ -52,10 +54,7 @@
     return pl.pallas_call(
         kernel,
         grid=(experts // per,),
-        in_specs=[
-            pl.BlockSpec((2, tok), lambda i: (0, 0)),
-            pl.BlockSpec((tok, half), lambda i: (0, 0)),
-        ],
+        in_specs=[SCALAR, ONCHIP, ONCHIP],
         out_specs=pl.BlockSpec((per * CAPACITY, half), lambda i: (i, 0)),
         out_shape=jax.ShapeDtypeStruct((experts * CAPACITY, half), BF16),
         scratch_shapes=[pltpu.VMEM((experts, tok), F32)],
@@ -64,9 +63,9 @@
             bytes_accessed=2 * (tok + experts * CAPACITY) * half,
             transcendentals=0,
         ),
-        compiler_params=pltpu.CompilerParams(vmem_limit_bytes=VMEM),
+        compiler_params=PARAMS,
         name="select_rows",
-    )(ids_t, tokens)
+    )(core, ids_t, tokens)
 
 
 def combine_matrix(ids_t, route_t, experts, after):
@@ -94,60 +93,49 @@
         out_specs=pl.BlockSpec((tok, rows), lambda: (0, 0)),
         out_shape=jax.ShapeDtypeStruct((tok, rows), BF16),
         cost_estimate=pl.CostEstimate(flops=4 * tok * rows, bytes_accessed=2 * tok * rows, transcendentals=0),
-        compiler_params=pltpu.CompilerParams(vmem_limit_bytes=VMEM),
+        compiler_params=PARAMS,
         name="combine_matrix",
     )(ids_t, route_t, after)
 
 
-def hidden_units(core, own, other, first, gain, w_gate, w_up):
-    rows, half = other.shape
+def hidden_units(core, own, other, gain, w_gate, w_up, first, length, after):
+    half = other.shape[1]
     units = w_gate.shape[1]
-    block = block_of(rows, 256)
-    skip = first // block
-
-    def kernel(core_ref, own_ref, other_ref, gain_a, gain_b, wg_a, wg_b, wu_a, wu_b, out_ref):
-        a = own_ref[...].astype(F32)
-        b = other_ref[...].astype(F32)
-        total = jnp.sum(a * a, axis=-1, keepdims=True) + jnp.sum(b * b, axis=-1, keepdims=True)
-        scale = lax.rsqrt(total * (1.0 / (2 * half)) + 1e-06)
-        na = (a * scale * gain_a[0]).astype(BF16)
-        nb = (b * scale * gain_b[0]).astype(BF16)
-        gate = jnp.dot(na, wg_a[0], preferred_element_type=F32) + jnp.dot(nb, wg_b[0], preferred_element_type=F32)
-        upper = jnp.dot(na, wu_a[0], preferred_element_type=F32) + jnp.dot(nb, wu_b[0], preferred_element_type=F32)
-        out_ref[...] = (gate / (1.0 + jnp.exp(-gate)) * upper).astype(BF16)
-
-    mine = lambda i, c: (c[0], 0, 0)
-    theirs = lambda i, c: (1 - c[0], 0, 0)
-    w_gate = w_gate.reshape(2, half, units)
-    w_up = w_up.reshape(2, half, units)
-    gain = gain.reshape(2, 1, half)
-    return pl.pallas_call(
-        kernel,
-        grid_spec=pltpu.PrefetchScalarGridSpec(
-            num_scalar_prefetch=1,
-            grid=(rows // block,),
-            in_specs=[
-                pl.BlockSpec((block, half), lambda i, c: (i + skip, 0)),
-                pl.BlockSpec((block, half), lambda i, c: (i, 0)),
-                pl.BlockSpec((1, 1, half), mine),
-                pl.BlockSpec((1, 1, half), theirs),
-                pl.BlockSpec((1, half, units), mine),
-                pl.BlockSpec((1, half, units), theirs),
-                pl.BlockSpec((1, half, units), mine),
-                pl.BlockSpec((1, half, units), theirs),
-            ],
-            out_specs=pl.BlockSpec((block, units), lambda i, c: (i, 0)),
-        ),
-        out_shape=jax.ShapeDtypeStruct((rows, units), BF16),
-        cost_estimate=pl.CostEstimate(
-            flops=8 * rows * half * units, bytes_accessed=4 * rows * half, transcendentals=rows * units
-        ),
-        compiler_params=pltpu.CompilerParams(vmem_limit_bytes=VMEM),
+    block = block_of(length, 256)
+
+    def kernel(core_ref, own_ref, other_ref, gain_ref, gate_ref, up_ref, *rest):
+        out_ref = rest[-1]
+        mine = core_ref[0]
+        theirs = 1 - mine
+        for start in range(0, length, block):
+            part = pl.ds(first + start, block)
+            a = own_ref[part, :].astype(F32)
+            b = other_ref[part, :].astype(F32)
+            total = jnp.sum(a * a + b * b, axis=-1, keepdims=True)
+            scale = lax.rsqrt(total * (1.0 / (2 * half)) + 1e-06)
+            a = (a * scale * gain_ref[mine]).astype(BF16)
+            b = (b * scale * gain_ref[theirs]).astype(BF16)
+            gate = jnp.dot(a, gate_ref[mine], preferred_element_type=F32)
+            gate = gate + jnp.dot(b, gate_ref[theirs], preferred_element_type=F32)
+            upper = jnp.dot(a, up_ref[mine], preferred_element_type=F32)
+            upper = upper + jnp.dot(b, up_ref[theirs], preferred_element_type=F32)
+            out_ref[pl.ds(start, block), :] = (gate / (1.0 + jnp.exp(-gate)) * upper).astype(BF16)
+
+    extra = [] if after is None else [after]
+    return pl.pallas_call(
+        kernel,
+        in_specs=[SCALAR] + [ONCHIP] * 5 + [ANY] * len(extra),
+        out_specs=ONCHIP,
+        out_shape=jax.ShapeDtypeStruct((length, units), BF16),
+        cost_estimate=pl.CostEstimate(
+            flops=8 * length * half * units, bytes_accessed=4 * length * half, transcendentals=length * units
+        ),
+        compiler_params=PARAMS,
         name="hidden_units",
-    )(core, own, other, gain, gain, w_gate, w_gate, w_up, w_up)
-
-
-def down_rows(core, own, other, first, w_down, total, result, after):
+    )(core, own, other, gain.reshape(2, 1, half), w_gate.reshape(2, half, units), w_up.reshape(2, half, units), *extra)
+
+
+def down_rows(core, own, other, first, w_down, total, result):
     rows, units = own.shape
     half = w_down.shape[1]
     block = block_of(rows, 256)
@@ -167,9 +155,6 @@
         pl.BlockSpec((1, units, half), lambda i, c: (1 - c[0], 0, 0)),
     ]
     aliases = {}
-    if after is not None:
-        operands.append(after)
-        in_specs.append(ANY)
     if result is not None:
         aliases = {len(operands): 0}
         operands.append(result)
@@ -187,7 +172,7 @@
         cost_estimate=pl.CostEstimate(
             flops=4 * rows * half * units, bytes_accessed=2 * rows * (half + 2 * units), transcendentals=0
         ),
-        compiler_params=pltpu.CompilerParams(vmem_limit_bytes=VMEM),
+        compiler_params=PARAMS,
         name="down_rows",
     )(*operands)
 
@@ -198,21 +183,22 @@
     block = 256
 
     def kernel(weights_ref, back_ref, out_ref):
-        out_ref[...] = jnp.dot(weights_ref[...], back_ref[...], preferred_element_type=F32).astype(BF16)
+        cols = pl.ds(pl.multiple_of(pl.program_id(0) * block, block), block)
+        out_ref[...] = jnp.dot(weights_ref[...], back_ref[:, cols], preferred_element_type=F32).astype(BF16)
 
     return pl.pallas_call(
         kernel,
         grid=(half // block,),
         in_specs=[
-            pl.BlockSpec((tok, rows), lambda i: (0, 0)),
-            pl.BlockSpec((rows, block), lambda i: (0, i)),
+            ONCHIP,
+            ONCHIP,
         ],
         out_specs=pl.BlockSpec((tok, block), lambda i: (0, i)),
         out_shape=jax.ShapeDtypeStruct((tok, half), BF16),
         cost_estimate=pl.CostEstimate(
             flops=2 * tok * rows * half, bytes_accessed=2 * (rows * (half + tok) + tok * half), transcendentals=0
         ),
-        compiler_params=pltpu.CompilerParams(vmem_limit_bytes=VMEM),
+        compiler_params=PARAMS,
         name="combine",
     )(weights, back)
 
@@ -231,19 +217,19 @@
         array = lax.all_to_all(array, "ep", split_axis=0, concat_axis=0, tiled=True)
         return array.reshape(rows, half)
 
-    own = exchange(select_rows(ids_t, tokens, experts))
+    own = exchange(select_rows(core, ids_t, tokens, experts))
+    other = lax.ppermute(own, "tp", swap)
+    weights = combine_matrix(ids_t, route_t, experts, own)
     length = rows // PIECES
+    result = None
     starts = range(0, rows, length)
-    others = [lax.ppermute(own[first : first + length], "tp", swap) for first in starts]
-    weights = combine_matrix(ids_t, route_t, experts, own)
     hidden = [
-        hidden_units(core, own, other, first, norm_gain, w_gate, w_up) for first, other in zip(starts, others)
+        hidden_units(core, own, other, norm_gain, w_gate, w_up, first, length, weights if first == 0 else None)
+        for first in starts
     ]
     crossed = [lax.ppermute(piece, "tp", swap) for piece in hidden]
-    result = None
     for first, mine, theirs in zip(starts, hidden, crossed):
-        after = weights if result is None else None
-        result = down_rows(core, mine, theirs, first, w_down, rows, result, after)
+        result = down_rows(core, mine, theirs, first, w_down, rows, result)
     return combine(weights, exchange(result))
 
 

time: 210 us -> 203 us (0.967)
  Pallas kernels: 18.8 us -> 14.6 us
  local copies, waits for them, and re-layouts: 6.13 us -> 1.94 us
  waiting for transfers between devices: 2.5 us -> 4.66 us
    pallas_call x5, Pallas kernels: 15 us -> 10.9 us  [the longest x3 5.15 us: hidden_units(): pl.pallas_call(kernel, in_specs=[SCALAR] + [ONCHIP] * 5 + [ANY] * len(ext...]
    unnamed x18 -> x16, local copies, waits for them, and re-layouts: 4.39 us -> 1.94 us
    ppermute x3 -> x1, waiting for transfers between devices: 2.49 us -> 4.65 us  [on_device(): other = lax.ppermute(own, 'tp', swap)]
  transfers between devices with their start and end apart: 6 -> 4, of which waited for: 1 -> 1; matrix products, arithmetic and copies ran while one was open for 0% -> 0% of each run, Pallas kernels for 6% -> 3%
where the time goes in v3:
time: 203 us
  blocking collectives  181 us (89%)
  Pallas kernels  14.6 us (7%)
  waiting for transfers between devices  4.66 us (2%)
    all_to_all x2, blocking collectives, exchange(): array = lax.all_to_all(array, 'ep', split_axis=0, concat_axis=0, tiled=True)  181 us
    pallas_call x3, Pallas kernels, hidden_units(): pl.pallas_call(kernel, in_specs=[SCALAR] + [ONCHIP] * 5 + [ANY] * len(ext...  5.15 us
    ppermute x1, waiting for transfers between devices, on_device(): other = lax.ppermute(own, 'tp', swap)  4.65 us
  transfers between devices with their start and end apart: 4, of which 1 were waited for; matrix products, arithmetic and copies ran while one was open for 0% of the time, Pallas kernels for 3%

profile of v3, /device:TPU:646, one launch (start us, length us, event | category | flops | bytes accessed | tf_op | source)
XLA Modules:
  0.0 203.1 jit_solution(6716279910914609317)
XLA Ops:
  0.0 0.0 copy-start.4
  0.0 0.7 copy-done.4
  0.7 0.0 copy-start.7
  0.7 1.2 copy-done.7
  1.9 2.5 %select_rows.1 = bf16[1536,1024]{1,0:T(8,128)(2,1)S(1)} custom-call(s32[1]{0:T(128)} %bitcast.2.core_ref, s32[2,512]{1,0:T(2,128)S(1)} %bitcast.34, bf16[512,1024]{1,0:T(8,128)(2,1)S(1)} %copy-done.7), custom_call_target="tpu_custom_call" | custom-call | flops 1610612736 | bytes 4194304 | tf_op jit(solution)/shard_map/select_rows/pallas_call | solution.py:54
  4.5 0.0 copy-start.5
  4.5 0.0 copy-start.6
  4.5 95.4 %all_to_all.10 = bf16[64,24,1024]{2,1,0:T(8,128)(2,1)S(1)} all-to-all(bf16[64,24,1024]{2,1,0:T(8,128)(2,1)S(1)} %bitcast.30), channel_id=1, replica_groups=mesh['grp'=2,'ep'=64,'tp'=2] {'ep'}, dimensions={0} | all-to-all | bytes 6291456 | tf_op jit(solution)/shard_map/all_to_all | solution.py:217
  99.9 0.0 collective-permute-start
  100.0 0.0 copy-done.5
  100.0 0.0 copy-done.6
  100.0 1.0 combine_matrix.1.rest_0_.weights_ref
  100.9 4.7 %collective-permute-done.other_ref = bf16[1536,1024]{1,0:T(8,128)(2,1)S(1)} collective-permute-done((bf16[1536,1024]{1,0:T(8,128)(2,1)S(1)}, bf16[1536,1024]{1,0:T(8,128)(2,1)S(1)}, u32[]{:S(2)}, u32[]{:S(2)}) %collective-permute-start) | collective-permute-done | bytes 3145760 | tf_op jit(solution)/shard_map/ppermute | solution.py:221
  105.6 0.0 copy-done.1
  105.6 0.0 copy-done.2
  105.6 0.0 copy-done.3
  105.6 1.7 hidden_units.5.own_ref
  107.3 0.3 collective-permute-start.3
  107.6 1.7 hidden_units.4.own_ref
  109.3 0.0 copy-start
  109.3 0.5 collective-permute-start.2
  109.8 1.7 hidden_units.3.own_ref
  111.5 0.3 collective-permute-start.1
  111.8 0.0 collective-permute-done.3.other_ref
  111.8 0.0 copy-done
  111.8 0.9 down_rows.3.rest_0_
  112.7 0.0 collective-permute-done.2.other_ref
  112.7 0.9 down_rows.4.rest_0_
  113.7 0.0 collective-permute-done.1.other_ref
  113.7 0.9 down_rows.5
  114.6 85.3 %all_to_all.11 = bf16[64,24,1024]{2,1,0:T(8,128)(2,1)S(1)} all-to-all(bf16[64,24,1024]{2,1,0:T(8,128)(2,1)S(1)} %bitcast.16), channel_id=1, replica_groups=mesh['grp'=2,'ep'=64,'tp'=2] {'ep'}, dimensions={0} | all-to-all | bytes 6291456 | tf_op jit(solution)/shard_map/all_to_all | solution.py:217
  199.9 3.2 %combine.1 = bf16[512,1024]{1,0:T(8,128)(2,1)} custom-call(bf16[512,1536]{1,0:T(8,128)(2,1)S(1)} %combine_matrix.1.rest_0_.weights_ref, bf16[1536,1024]{1,0:T(8,128)(2,1)S(1)} %bitcast.29), custom_call_target="tpu_custom_call" | custom-call | flops 1610612736 | bytes 5767168 | tf_op jit(solution)/shard_map/combine/pallas_call | solution.py:189
  (3 shorter events, 0.0 us)
Async XLA Ops:
  0.0 0.7 copy-start.4
  0.7 1.2 copy-start.7
  4.5 95.5 %copy-start.5 = (s32[512,2]{0,1:T(2,128)S(1)}, s32[512,2]{0,1:T(2,128)}, u32[]{:S(2)}) copy-start(s32[512,2]{0,1:T(2,128)} %param.9) | copy-start | bytes 12292
  4.5 95.5 %copy-start.6 = (f32[512,2]{0,1:T(2,128)S(1)}, f32[512,2]{0,1:T(2,128)}, u32[]{:S(2)}) copy-start(f32[512,2]{0,1:T(2,128)} %param.10) | copy-start | bytes 12292
  99.9 5.7 %copy-start.1 = (bf16[1,2048,256]{2,1,0:T(8,128)(2,1)S(1)}, bf16[1,2048,256]{2,1,0:T(8,128)(2,1)}, u32[]{:S(2)}) copy-start(bf16[1,2048,256]{2,1,0:T(8,128)(2,1)} %param.11) | copy-start | bytes 3145732
  99.9 5.7 %copy-start.2 = (bf16[1,2048,256]{2,1,0:T(8,128)(2,1)S(1)}, bf16[1,2048,256]{2,1,0:T(8,128)(2,1)}, u32[]{:S(2)}) copy-start(bf16[1,2048,256]{2,1,0:T(8,128)(2,1)} %param.12) | copy-start | bytes 3145732
  99.9 5.7 %copy-start.3 = (f32[2048]{0:T(1024)S(1)}, f32[2048]{0:T(1024)}, u32[]{:S(2)}) copy-start(f32[2048]{0:T(1024)} %param.8) | copy-start | bytes 24580
  99.9 5.7 %collective-permute-start = (bf16[1536,1024]{1,0:T(8,128)(2,1)S(1)}, bf16[1536,1024]{1,0:T(8,128)(2,1)S(1)}, u32[]{:S(2)}, u32[]{:S(2)}) collective-permute-start(bf16[1536,1024]{1,0:T(8,128)(2,1)S(1)} %bitcast.11), channel_id=1, source_target_pairs={{0,1},{1,0},{2,3},{3,2},{4,5},{5,4},{6,7},{7,6},{8,9},{9,8},{10,11... | collective-permute-start | bytes 9437192 | tf_op jit(solution)/shard_map/ppermute | solution.py:221
  107.3 4.5 %collective-permute-start.3 = (bf16[512,256]{1,0:T(8,128)(2,1)S(1)}, bf16[512,256]{1,0:T(8,128)(2,1)S(1)}, u32[]{:S(2)}, u32[]{:S(2)}) collective-permute-start(bf16[512,256]{1,0:T(8,128)(2,1)S(1)} %hidden_units.5.own_ref), channel_id=1, source_target_pairs={{0,1},{1,0},{2,3},{3,2},{4,5},{5,4},{6,7},{7,6},{8,9},{9,8},{10,11... | collective-permute-start | bytes 786440 | tf_op jit(solution)/shard_map/ppermute | solution.py:230
  109.3 2.5 %copy-start = (bf16[1,512,1024]{2,1,0:T(8,128)(2,1)S(1)}, bf16[1,512,1024]{2,1,0:T(8,128)(2,1)}, u32[]{:S(2)}) copy-start(bf16[1,512,1024]{2,1,0:T(8,128)(2,1)} %param.13) | copy-start | bytes 3145732
  109.3 3.4 %collective-permute-start.2 = (bf16[512,256]{1,0:T(8,128)(2,1)S(1)}, bf16[512,256]{1,0:T(8,128)(2,1)S(1)}, u32[]{:S(2)}, u32[]{:S(2)}) collective-permute-start(bf16[512,256]{1,0:T(8,128)(2,1)S(1)} %hidden_units.4.own_ref), channel_id=1, source_target_pairs={{0,1},{1,0},{2,3},{3,2},{4,5},{5,4},{6,7},{7,6},{8,9},{9,8},{10,11... | collective-permute-start | bytes 786440 | tf_op jit(solution)/shard_map/ppermute | solution.py:230
  111.5 2.1 %collective-permute-start.1 = (bf16[512,256]{1,0:T(8,128)(2,1)S(1)}, bf16[512,256]{1,0:T(8,128)(2,1)S(1)}, u32[]{:S(2)}, u32[]{:S(2)}) collective-permute-start(bf16[512,256]{1,0:T(8,128)(2,1)S(1)} %hidden_units.3.own_ref), channel_id=1, source_target_pairs={{0,1},{1,0},{2,3},{3,2},{4,5},{5,4},{6,7},{7,6},{8,9},{9,8},{10,11... | collective-permute-start | bytes 786440 | tf_op jit(solution)/shard_map/ppermute | solution.py:230

commit v4 on v3

--- a/solution.py
+++ b/solution.py
@@ -6,7 +6,8 @@
 from jax.sharding import PartitionSpec as P
 
 CAPACITY = 24
-PIECES = 3
+PIECES_OF = 6
+PIECE_ENDS = (2, 4, 6)
 PARAMS = pltpu.CompilerParams(vmem_limit_bytes=20 * 1024 * 1024)
 BF16 = jnp.bfloat16
 F32 = jnp.float32
@@ -98,8 +99,8 @@
     )(ids_t, route_t, after)
 
 
-def hidden_units(core, own, other, gain, w_gate, w_up, first, length, after):
-    half = other.shape[1]
+def hidden_units(core, own, other, gain, w_gate, w_up, first, after):
+    length, half = other.shape
     units = w_gate.shape[1]
     block = block_of(length, 256)
 
@@ -110,7 +111,7 @@
         for start in range(0, length, block):
             part = pl.ds(first + start, block)
             a = own_ref[part, :].astype(F32)
-            b = other_ref[part, :].astype(F32)
+            b = other_ref[pl.ds(start, block), :].astype(F32)
             total = jnp.sum(a * a + b * b, axis=-1, keepdims=True)
             scale = lax.rsqrt(total * (1.0 / (2 * half)) + 1e-06)
             a = (a * scale * gain_ref[mine]).astype(BF16)
@@ -135,52 +136,70 @@
     )(core, own, other, gain.reshape(2, 1, half), w_gate.reshape(2, half, units), w_up.reshape(2, half, units), *extra)
 
 
-def down_rows(core, own, other, first, w_down, total, result):
+def first_down_rows(core, own, other, starts, w_down, total):
+    units = own[0].shape[1]
+    half = w_down.shape[1]
+    count = len(own)
+
+    def kernel(core_ref, w_ref, *rest):
+        out_ref = rest[-1]
+        mine = core_ref[0]
+        theirs = 1 - mine
+        for n, first in enumerate(starts):
+            length = own[n].shape[0]
+            block = block_of(length, 256)
+            for start in range(0, length, block):
+                part = pl.ds(start, block)
+                out = jnp.dot(rest[n][part, :], w_ref[mine], preferred_element_type=F32)
+                out = out + jnp.dot(rest[count + n][part, :], w_ref[theirs], preferred_element_type=F32)
+                out_ref[pl.ds(first + start, block), :] = out.astype(BF16)
+
+    rows = sum(piece.shape[0] for piece in own)
+    return pl.pallas_call(
+        kernel,
+        in_specs=[SCALAR] + [ONCHIP] * (1 + 2 * count),
+        out_specs=ONCHIP,
+        out_shape=jax.ShapeDtypeStruct((total, half), BF16),
+        cost_estimate=pl.CostEstimate(
+            flops=4 * rows * half * units, bytes_accessed=2 * rows * (half + 2 * units), transcendentals=0
+        ),
+        compiler_params=PARAMS,
+        name="first_down_rows",
+    )(core, w_down.reshape(2, units, half), *own, *other)
+
+
+def last_down_rows(core, own, other, first, w_down, result):
     rows, units = own.shape
-    half = w_down.shape[1]
+    total, half = result.shape
     block = block_of(rows, 256)
     skip = first // block
 
-    def kernel(core_ref, own_ref, other_ref, w_a, w_b, *rest):
-        out = jnp.dot(own_ref[...], w_a[0], preferred_element_type=F32)
-        out = out + jnp.dot(other_ref[...], w_b[0], preferred_element_type=F32)
-        rest[-1][...] = out.astype(BF16)
-
-    w_down = w_down.reshape(2, units, half)
-    operands = [core, own, other, w_down, w_down]
-    in_specs = [
-        pl.BlockSpec((block, units), lambda i, c: (i, 0)),
-        pl.BlockSpec((block, units), lambda i, c: (i, 0)),
-        pl.BlockSpec((1, units, half), lambda i, c: (c[0], 0, 0)),
-        pl.BlockSpec((1, units, half), lambda i, c: (1 - c[0], 0, 0)),
-    ]
-    aliases = {}
-    if result is not None:
-        aliases = {len(operands): 0}
-        operands.append(result)
-        in_specs.append(ANY)
-    return pl.pallas_call(
-        kernel,
-        grid_spec=pltpu.PrefetchScalarGridSpec(
-            num_scalar_prefetch=1,
-            grid=(rows // block,),
-            in_specs=in_specs,
-            out_specs=pl.BlockSpec((block, half), lambda i, c: (i + skip, 0)),
-        ),
+    def kernel(core_ref, own_ref, other_ref, w_ref, result_ref, out_ref):
+        mine = core_ref[0]
+        part = pl.ds(pl.multiple_of(pl.program_id(0) * block, block), block)
+        out = jnp.dot(own_ref[part, :], w_ref[mine], preferred_element_type=F32)
+        out = out + jnp.dot(other_ref[part, :], w_ref[1 - mine], preferred_element_type=F32)
+        out_ref[...] = out.astype(BF16)
+
+    return pl.pallas_call(
+        kernel,
+        grid=(rows // block,),
+        in_specs=[SCALAR, ONCHIP, ONCHIP, ONCHIP, ANY],
+        out_specs=pl.BlockSpec((block, half), lambda i: (i + skip, 0)),
         out_shape=jax.ShapeDtypeStruct((total, half), BF16),
-        input_output_aliases=aliases,
+        input_output_aliases={4: 0},
         cost_estimate=pl.CostEstimate(
             flops=4 * rows * half * units, bytes_accessed=2 * rows * (half + 2 * units), transcendentals=0
         ),
         compiler_params=PARAMS,
-        name="down_rows",
-    )(*operands)
+        name="last_down_rows",
+    )(core, own, other, w_down.reshape(2, units, half), result)
 
 
 def combine(weights, back):
     tok, rows = weights.shape
     half = back.shape[1]
-    block = 256
+    block = half // 2
 
     def kernel(weights_ref, back_ref, out_ref):
         cols = pl.ds(pl.multiple_of(pl.program_id(0) * block, block), block)
@@ -218,18 +237,17 @@
         return array.reshape(rows, half)
 
     own = exchange(select_rows(core, ids_t, tokens, experts))
-    other = lax.ppermute(own, "tp", swap)
     weights = combine_matrix(ids_t, route_t, experts, own)
-    length = rows // PIECES
-    result = None
-    starts = range(0, rows, length)
+    ends = [rows * n // PIECES_OF for n in PIECE_ENDS]
+    starts = [0] + ends[:-1]
+    others = [lax.ppermute(own[first:end], "tp", swap) for first, end in zip(starts, ends)]
     hidden = [
-        hidden_units(core, own, other, norm_gain, w_gate, w_up, first, length, weights if first == 0 else None)
-        for first in starts
+        hidden_units(core, own, other, norm_gain, w_gate, w_up, first, weights if first == 0 else None)
+        for first, other in zip(starts, others)
     ]
     crossed = [lax.ppermute(piece, "tp", swap) for piece in hidden]
-    for first, mine, theirs in zip(starts, hidden, crossed):
-        result = down_rows(core, mine, theirs, first, w_down, rows, result)
+    result = first_down_rows(core, hidden[:-1], crossed[:-1], starts[:-1], w_down, rows)
+    result = last_down_rows(core, hidden[-1], crossed[-1], starts[-1], w_down, result)
     return combine(weights, exchange(result))
 
 

time: 203 us -> 199 us (0.980)
  waiting for transfers between devices: 4.66 us -> 1.15 us
    ppermute x1 -> x3, waiting for transfers between devices: 4.65 us -> 1.03 us  [on_device(): lax.ppermute(own[first:end], 'tp', swap)]
  transfers between devices with their start and end apart: 4 -> 6, of which waited for: 1 -> 2; matrix products, arithmetic and copies ran while one was open for 0% -> 0% of each run, Pallas kernels for 3% -> 4%
where the time goes in v4:
time: 199 us
  blocking collectives  180 us (90%)
  Pallas kernels  13.6 us (7%)
  local copies, waits for them, and re-layouts  2.25 us (1%)
    all_to_all x2, blocking collectives, exchange(): array = lax.all_to_all(array, 'ep', split_axis=0, concat_axis=0, tiled=True)  180 us
    pallas_call x3, Pallas kernels, hidden_units(): pl.pallas_call(kernel, in_specs=[SCALAR] + [ONCHIP] * 5 + [ANY] * len(ext...  5.15 us
  transfers between devices with their start and end apart: 6, of which 2 were waited for; matrix products, arithmetic and copies ran while one was open for 0% of the time, Pallas kernels for 4%

profile of v4, /device:TPU:646, one launch (start us, length us, event | category | flops | bytes accessed | tf_op | source)
XLA Modules:
  0.0 198.7 jit_solution(15260373320890996394)
XLA Ops:
  0.0 0.7 copy-done.4
  0.7 1.2 copy-done.7
  1.9 2.5 %select_rows.1 = bf16[1536,1024]{1,0:T(8,128)(2,1)S(1)} custom-call(s32[1]{0:T(128)} %bitcast.2.core_ref, s32[2,512]{1,0:T(2,128)S(1)} %bitcast.30, bf16[512,1024]{1,0:T(8,128)(2,1)S(1)} %copy-done.7), custom_call_target="tpu_custom_call" | custom-call | flops 1610612736 | bytes 4194304 | tf_op jit(solution)/shard_map/select_rows/pallas_call | solution.py:55
  4.5 95.4 %all_to_all.10 = bf16[64,24,1024]{2,1,0:T(8,128)(2,1)S(1)} all-to-all(bf16[64,24,1024]{2,1,0:T(8,128)(2,1)S(1)} %bitcast.26), channel_id=1, replica_groups=mesh['grp'=2,'ep'=64,'tp'=2] {'ep'}, dimensions={0} | all-to-all | bytes 6291456 | tf_op jit(solution)/shard_map/all_to_all | solution.py:236
  99.9 0.3 fusion
  100.2 0.0 copy-start
  100.2 0.0 copy-start.1
  100.2 0.0 copy-start.3
  100.3 0.1 collective-permute-start.3
  100.4 0.5 collective-permute-start.2
  100.9 0.1 collective-permute-start
  101.0 0.0 copy-done.5
  101.0 1.0 combine_matrix.1.rest_0_.weights_ref
  102.0 1.0 collective-permute-done.3.other_ref
  103.0 0.0 copy-done
  103.0 0.0 copy-done.3
  103.1 1.7 hidden_units.5.rest_1_
  104.8 0.3 collective-permute-start.5
  105.0 0.0 collective-permute-done.2.other_ref
  105.0 1.7 hidden_units.4.rest_0_
  106.8 0.0 copy-start.2
  106.8 0.5 collective-permute-start.4
  107.3 0.0 collective-permute-done.other_ref
  107.3 1.7 hidden_units.3.own_ref
  109.0 0.4 collective-permute-start.1
  109.4 0.0 collective-permute-done.5.rest_3_
  109.4 0.0 collective-permute-done.4.rest_2_
  109.4 1.3 first_down_rows.1.result_ref
  110.7 0.1 collective-permute-done.1.other_ref
  110.8 0.9 last_down_rows.1
  111.7 84.2 %all_to_all.11 = bf16[64,24,1024]{2,1,0:T(8,128)(2,1)S(1)} all-to-all(bf16[64,24,1024]{2,1,0:T(8,128)(2,1)S(1)} %bitcast.16), channel_id=1, replica_groups=mesh['grp'=2,'ep'=64,'tp'=2] {'ep'}, dimensions={0} | all-to-all | bytes 6291456 | tf_op jit(solution)/shard_map/all_to_all | solution.py:236
  195.9 2.8 %combine.1 = bf16[512,1024]{1,0:T(8,128)(2,1)} custom-call(bf16[512,1536]{1,0:T(8,128)(2,1)S(1)} %combine_matrix.1.rest_0_.weights_ref, bf16[1536,1024]{1,0:T(8,128)(2,1)S(1)} %bitcast.25), custom_call_target="tpu_custom_call" | custom-call | flops 1610612736 | bytes 5767168 | tf_op jit(solution)/shard_map/combine/pallas_call | solution.py:208
  (7 shorter events, 0.0 us)
Async XLA Ops:
  0.0 0.7 copy-start.4
  0.7 1.2 copy-start.7
  99.9 1.1 copy-start.5
  99.9 1.1 copy-start.6
  100.2 2.8 %copy-start = (bf16[1,2048,256]{2,1,0:T(8,128)(2,1)S(1)}, bf16[1,2048,256]{2,1,0:T(8,128)(2,1)}, u32[]{:S(2)}) copy-start(bf16[1,2048,256]{2,1,0:T(8,128)(2,1)} %param.11) | copy-start | bytes 3145732
  100.2 2.8 %copy-start.1 = (bf16[1,2048,256]{2,1,0:T(8,128)(2,1)S(1)}, bf16[1,2048,256]{2,1,0:T(8,128)(2,1)}, u32[]{:S(2)}) copy-start(bf16[1,2048,256]{2,1,0:T(8,128)(2,1)} %param.12) | copy-start | bytes 3145732
  100.2 2.8 %copy-start.3 = (f32[2048]{0:T(1024)S(1)}, f32[2048]{0:T(1024)}, u32[]{:S(2)}) copy-start(f32[2048]{0:T(1024)} %param.8) | copy-start | bytes 24580
  100.3 2.8 %collective-permute-start.3 = (bf16[512,1024]{1,0:T(8,128)(2,1)S(1)}, bf16[512,1024]{1,0:T(8,128)(2,1)S(1)}, u32[]{:S(2)}, u32[]{:S(2)}) collective-permute-start(bf16[512,1024]{1,0:T(8,128)(2,1)S(1)} %get-tuple-element.5), channel_id=1, source_target_pairs={{0,1},{1,0},{2,3},{3,2},{4,5},{5,4},{6,7},{7,6},{8,9},{9,8},{10,11... | collective-permute-start | bytes 3145736 | tf_op jit(solution)/shard_map/ppermute | solution.py:243
  100.4 4.6 %collective-permute-start.2 = (bf16[512,1024]{1,0:T(8,128)(2,1)S(1)}, bf16[512,1024]{1,0:T(8,128)(2,1)S(1)}, u32[]{:S(2)}, u32[]{:S(2)}) collective-permute-start(bf16[512,1024]{1,0:T(8,128)(2,1)S(1)} %get-tuple-element.6), channel_id=1, source_target_pairs={{0,1},{1,0},{2,3},{3,2},{4,5},{5,4},{6,7},{7,6},{8,9},{9,8},{10,11... | collective-permute-start | bytes 3145736 | tf_op jit(solution)/shard_map/ppermute | solution.py:243
  100.9 6.4 %collective-permute-start = (bf16[512,1024]{1,0:T(8,128)(2,1)S(1)}, bf16[512,1024]{1,0:T(8,128)(2,1)S(1)}, u32[]{:S(2)}, u32[]{:S(2)}) collective-permute-start(bf16[512,1024]{1,0:T(8,128)(2,1)S(1)} %get-tuple-element.7), channel_id=1, source_target_pairs={{0,1},{1,0},{2,3},{3,2},{4,5},{5,4},{6,7},{7,6},{8,9},{9,8},{10,11... | collective-permute-start | bytes 3145736 | tf_op jit(solution)/shard_map/ppermute | solution.py:243
  104.8 4.7 %collective-permute-start.5 = (bf16[512,256]{1,0:T(8,128)(2,1)S(1)}, bf16[512,256]{1,0:T(8,128)(2,1)S(1)}, u32[]{:S(2)}, u32[]{:S(2)}) collective-permute-start(bf16[512,256]{1,0:T(8,128)(2,1)S(1)} %hidden_units.5.rest_1_), channel_id=1, source_target_pairs={{0,1},{1,0},{2,3},{3,2},{4,5},{5,4},{6,7},{7,6},{8,9},{9,8},{10,11... | collective-permute-start | bytes 786440 | tf_op jit(solution)/shard_map/ppermute | solution.py:248
  106.8 2.7 %copy-start.2 = (bf16[1,512,1024]{2,1,0:T(8,128)(2,1)S(1)}, bf16[1,512,1024]{2,1,0:T(8,128)(2,1)}, u32[]{:S(2)}) copy-start(bf16[1,512,1024]{2,1,0:T(8,128)(2,1)} %param.13) | copy-start | bytes 3145732
  106.8 2.7 %collective-permute-start.4 = (bf16[512,256]{1,0:T(8,128)(2,1)S(1)}, bf16[512,256]{1,0:T(8,128)(2,1)S(1)}, u32[]{:S(2)}, u32[]{:S(2)}) collective-permute-start(bf16[512,256]{1,0:T(8,128)(2,1)S(1)} %hidden_units.4.rest_0_), channel_id=1, source_target_pairs={{0,1},{1,0},{2,3},{3,2},{4,5},{5,4},{6,7},{7,6},{8,9},{9,8},{10,11... | collective-permute-start | bytes 786440 | tf_op jit(solution)/shard_map/ppermute | solution.py:248
  109.0 1.8 collective-permute-start.1

commit v5 on v4

--- a/solution.py
+++ b/solution.py
@@ -39,26 +39,22 @@
     tok, half = tokens.shape
     per = block_of(experts, 16)
 
-    def kernel(core_ref, ids_ref, tok_ref, out_ref, key_ref):
-        step = pl.program_id(0)
-
-        @pl.when(step == 0)
-        def _():
-            _, named, slot = slots_of(ids_ref, experts)
-            key_ref[...] = jnp.where(named, slot, -1.0)
-
-        key = key_ref[pl.ds(pl.multiple_of(step * per, per), per), :]
+    def kernel(core_ref, ids_ref, tok_ref, out_ref):
+        _, named, slot = slots_of(ids_ref, experts)
+        keys = jnp.where(named, slot, -1.0)
         wanted = lax.broadcasted_iota(jnp.int32, (per, CAPACITY, tok), 1).astype(F32)
-        chosen = jnp.where(key[:, None, :] == wanted, 1.0, 0.0).reshape(per * CAPACITY, tok).astype(BF16)
-        out_ref[...] = jnp.dot(chosen, tok_ref[...], preferred_element_type=F32).astype(BF16)
-
-    return pl.pallas_call(
-        kernel,
-        grid=(experts // per,),
+        for first in range(0, experts, per):
+            key = keys[first : first + per]
+            chosen = jnp.where(key[:, None, :] == wanted, 1.0, 0.0).reshape(per * CAPACITY, tok).astype(BF16)
+            out_ref[pl.ds(first * CAPACITY, per * CAPACITY), :] = jnp.dot(
+                chosen, tok_ref[...], preferred_element_type=F32
+            ).astype(BF16)
+
+    return pl.pallas_call(
+        kernel,
         in_specs=[SCALAR, ONCHIP, ONCHIP],
-        out_specs=pl.BlockSpec((per * CAPACITY, half), lambda i: (i, 0)),
+        out_specs=ONCHIP,
         out_shape=jax.ShapeDtypeStruct((experts * CAPACITY, half), BF16),
-        scratch_shapes=[pltpu.VMEM((experts, tok), F32)],
         cost_estimate=pl.CostEstimate(
             flops=2 * experts * CAPACITY * tok * half,
             bytes_accessed=2 * (tok + experts * CAPACITY) * half,

time: 199 us -> 199 us (level)
  no operation moved by 1% of the time
where the time goes in v5:
time: 199 us
  blocking collectives  180 us (90%)
  Pallas kernels  13.1 us (7%)
  local copies, waits for them, and re-layouts  2.25 us (1%)
    all_to_all x2, blocking collectives, exchange(): array = lax.all_to_all(array, 'ep', split_axis=0, concat_axis=0, tiled=True)  180 us
    pallas_call x3, Pallas kernels, hidden_units(): pl.pallas_call(kernel, in_specs=[SCALAR] + [ONCHIP] * 5 + [ANY] * len(ext...  5.15 us
  transfers between devices with their start and end apart: 6, of which 2 were waited for; matrix products, arithmetic and copies ran while one was open for 0% of the time, Pallas kernels for 4%

profile of v5, /device:TPU:646, one launch (start us, length us, event | category | flops | bytes accessed | tf_op | source)
XLA Modules:
  0.0 198.7 jit_solution(10130179151024440560)
XLA Ops:
  0.0 0.7 copy-done.4
  0.7 1.2 copy-done.7
  1.9 2.0 %select_rows.1 = bf16[1536,1024]{1,0:T(8,128)(2,1)S(1)} custom-call(s32[1]{0:T(128)} %bitcast.2.core_ref, s32[2,512]{1,0:T(2,128)S(1)} %bitcast.30, bf16[512,1024]{1,0:T(8,128)(2,1)S(1)} %copy-done.7), custom_call_target="tpu_custom_call" | custom-call | flops 1610612736 | bytes 4194304 | tf_op jit(solution)/shard_map/select_rows/pallas_call | solution.py:53
  3.9 95.4 %all_to_all.10 = bf16[64,24,1024]{2,1,0:T(8,128)(2,1)S(1)} all-to-all(bf16[64,24,1024]{2,1,0:T(8,128)(2,1)S(1)} %bitcast.26), channel_id=1, replica_groups=mesh['grp'=2,'ep'=64,'tp'=2] {'ep'}, dimensions={0} | all-to-all | bytes 6291456 | tf_op jit(solution)/shard_map/all_to_all | solution.py:232
  99.4 0.3 fusion
  99.7 0.0 copy-start
  99.7 0.0 copy-start.1
  99.7 0.0 copy-start.3
  99.7 0.1 collective-permute-start.3
  99.9 0.5 collective-permute-start.2
  100.3 0.1 collective-permute-start
  100.5 0.0 copy-done.5
  100.5 0.0 copy-done.6
  100.5 1.0 combine_matrix.1.rest_0_.weights_ref
  101.5 1.0 collective-permute-done.3.other_ref
  102.5 0.0 copy-done.3
  102.5 1.7 hidden_units.5.rest_1_
  104.2 0.3 collective-permute-start.5
  104.5 0.0 collective-permute-done.2.other_ref
  104.5 1.7 hidden_units.4.rest_0_
  106.2 0.0 copy-start.2
  106.2 0.7 collective-permute-start.4
  106.9 0.0 collective-permute-done.other_ref
  106.9 1.7 hidden_units.3.own_ref
  108.6 0.3 collective-permute-start.1
  108.9 0.0 collective-permute-done.5.rest_3_
  108.9 0.0 collective-permute-done.4.rest_2_
  108.9 1.3 first_down_rows.1.result_ref
  110.2 0.1 collective-permute-done.1.other_ref
  110.3 0.9 last_down_rows.1
  111.2 84.7 %all_to_all.11 = bf16[64,24,1024]{2,1,0:T(8,128)(2,1)S(1)} all-to-all(bf16[64,24,1024]{2,1,0:T(8,128)(2,1)S(1)} %bitcast.16), channel_id=1, replica_groups=mesh['grp'=2,'ep'=64,'tp'=2] {'ep'}, dimensions={0} | all-to-all | bytes 6291456 | tf_op jit(solution)/shard_map/all_to_all | solution.py:232
  195.9 2.8 %combine.1 = bf16[512,1024]{1,0:T(8,128)(2,1)} custom-call(bf16[512,1536]{1,0:T(8,128)(2,1)S(1)} %combine_matrix.1.rest_0_.weights_ref, bf16[1536,1024]{1,0:T(8,128)(2,1)S(1)} %bitcast.25), custom_call_target="tpu_custom_call" | custom-call | flops 1610612736 | bytes 5767168 | tf_op jit(solution)/shard_map/combine/pallas_call | solution.py:204
  (7 shorter events, 0.0 us)
Async XLA Ops:
  0.0 0.7 copy-start.4
  0.7 1.2 copy-start.7
  99.4 1.1 copy-start.5
  99.4 1.1 copy-start.6
  99.7 2.8 %copy-start = (bf16[1,2048,256]{2,1,0:T(8,128)(2,1)S(1)}, bf16[1,2048,256]{2,1,0:T(8,128)(2,1)}, u32[]{:S(2)}) copy-start(bf16[1,2048,256]{2,1,0:T(8,128)(2,1)} %param.11) | copy-start | bytes 3145732
  99.7 2.8 %copy-start.1 = (bf16[1,2048,256]{2,1,0:T(8,128)(2,1)S(1)}, bf16[1,2048,256]{2,1,0:T(8,128)(2,1)}, u32[]{:S(2)}) copy-start(bf16[1,2048,256]{2,1,0:T(8,128)(2,1)} %param.12) | copy-start | bytes 3145732
  99.7 2.8 %copy-start.3 = (f32[2048]{0:T(1024)S(1)}, f32[2048]{0:T(1024)}, u32[]{:S(2)}) copy-start(f32[2048]{0:T(1024)} %param.8) | copy-start | bytes 24580
  99.7 2.8 %collective-permute-start.3 = (bf16[512,1024]{1,0:T(8,128)(2,1)S(1)}, bf16[512,1024]{1,0:T(8,128)(2,1)S(1)}, u32[]{:S(2)}, u32[]{:S(2)}) collective-permute-start(bf16[512,1024]{1,0:T(8,128)(2,1)S(1)} %get-tuple-element.5), channel_id=1, source_target_pairs={{0,1},{1,0},{2,3},{3,2},{4,5},{5,4},{6,7},{7,6},{8,9},{9,8},{10,11... | collective-permute-start | bytes 3145736 | tf_op jit(solution)/shard_map/ppermute | solution.py:239
  99.9 4.6 %collective-permute-start.2 = (bf16[512,1024]{1,0:T(8,128)(2,1)S(1)}, bf16[512,1024]{1,0:T(8,128)(2,1)S(1)}, u32[]{:S(2)}, u32[]{:S(2)}) collective-permute-start(bf16[512,1024]{1,0:T(8,128)(2,1)S(1)} %get-tuple-element.6), channel_id=1, source_target_pairs={{0,1},{1,0},{2,3},{3,2},{4,5},{5,4},{6,7},{7,6},{8,9},{9,8},{10,11... | collective-permute-start | bytes 3145736 | tf_op jit(solution)/shard_map/ppermute | solution.py:239
  100.3 6.6 %collective-permute-start = (bf16[512,1024]{1,0:T(8,128)(2,1)S(1)}, bf16[512,1024]{1,0:T(8,128)(2,1)S(1)}, u32[]{:S(2)}, u32[]{:S(2)}) collective-permute-start(bf16[512,1024]{1,0:T(8,128)(2,1)S(1)} %get-tuple-element.7), channel_id=1, source_target_pairs={{0,1},{1,0},{2,3},{3,2},{4,5},{5,4},{6,7},{7,6},{8,9},{9,8},{10,11... | collective-permute-start | bytes 3145736 | tf_op jit(solution)/shard_map/ppermute | solution.py:239
  104.2 4.7 %collective-permute-start.5 = (bf16[512,256]{1,0:T(8,128)(2,1)S(1)}, bf16[512,256]{1,0:T(8,128)(2,1)S(1)}, u32[]{:S(2)}, u32[]{:S(2)}) collective-permute-start(bf16[512,256]{1,0:T(8,128)(2,1)S(1)} %hidden_units.5.rest_1_), channel_id=1, source_target_pairs={{0,1},{1,0},{2,3},{3,2},{4,5},{5,4},{6,7},{7,6},{8,9},{9,8},{10,11... | collective-permute-start | bytes 786440 | tf_op jit(solution)/shard_map/ppermute | solution.py:244
  106.2 2.7 %copy-start.2 = (bf16[1,512,1024]{2,1,0:T(8,128)(2,1)S(1)}, bf16[1,512,1024]{2,1,0:T(8,128)(2,1)}, u32[]{:S(2)}) copy-start(bf16[1,512,1024]{2,1,0:T(8,128)(2,1)} %param.13) | copy-start | bytes 3145732
  106.2 2.7 %collective-permute-start.4 = (bf16[512,256]{1,0:T(8,128)(2,1)S(1)}, bf16[512,256]{1,0:T(8,128)(2,1)S(1)}, u32[]{:S(2)}, u32[]{:S(2)}) collective-permute-start(bf16[512,256]{1,0:T(8,128)(2,1)S(1)} %hidden_units.4.rest_0_), channel_id=1, source_target_pairs={{0,1},{1,0},{2,3},{3,2},{4,5},{5,4},{6,7},{7,6},{8,9},{9,8},{10,11... | collective-permute-start | bytes 786440 | tf_op jit(solution)/shard_map/ppermute | solution.py:244
  108.6 1.7 collective-permute-start.1

commit v6 on v5

--- a/solution.py
+++ b/solution.py
@@ -95,7 +95,7 @@
     )(ids_t, route_t, after)
 
 
-def hidden_units(core, own, other, gain, w_gate, w_up, first, after):
+def hidden_units(core, own, other, gain, w_gate, w_up, first, room, after, result):
     length, half = other.shape
     units = w_gate.shape[1]
     block = block_of(length, 256)
@@ -118,12 +118,16 @@
             upper = upper + jnp.dot(b, up_ref[theirs], preferred_element_type=F32)
             out_ref[pl.ds(start, block), :] = (gate / (1.0 + jnp.exp(-gate)) * upper).astype(BF16)
 
-    extra = [] if after is None else [after]
-    return pl.pallas_call(
-        kernel,
+    extra = [x for x in (after, result) if x is not None]
+    aliases = {} if result is None else {5 + len(extra): 0}
+    out_spec = ONCHIP if result is None else pl.BlockSpec((length, units), lambda i: (first // length, 0))
+    return pl.pallas_call(
+        kernel,
+        grid=() if result is None else (1,),
         in_specs=[SCALAR] + [ONCHIP] * 5 + [ANY] * len(extra),
-        out_specs=ONCHIP,
-        out_shape=jax.ShapeDtypeStruct((length, units), BF16),
+        out_specs=out_spec,
+        out_shape=jax.ShapeDtypeStruct((room, units), BF16),
+        input_output_aliases=aliases,
         cost_estimate=pl.CostEstimate(
             flops=8 * length * half * units, bytes_accessed=4 * length * half, transcendentals=length * units
         ),
@@ -195,21 +199,24 @@
 def combine(weights, back):
     tok, rows = weights.shape
     half = back.shape[1]
-    block = half // 2
-
-    def kernel(weights_ref, back_ref, out_ref):
-        cols = pl.ds(pl.multiple_of(pl.program_id(0) * block, block), block)
-        out_ref[...] = jnp.dot(weights_ref[...], back_ref[:, cols], preferred_element_type=F32).astype(BF16)
-
-    return pl.pallas_call(
-        kernel,
-        grid=(half // block,),
-        in_specs=[
-            ONCHIP,
-            ONCHIP,
-        ],
-        out_specs=pl.BlockSpec((tok, block), lambda i: (0, i)),
+    block = 256
+
+    def kernel(weights_ref, back_ref, out_hbm, out_ref, sems):
+        copies = []
+        for n in range(half // block):
+            cols = pl.ds(n * block, block)
+            out_ref[:, cols] = jnp.dot(weights_ref[...], back_ref[:, cols], preferred_element_type=F32).astype(BF16)
+            copies.append(pltpu.make_async_copy(out_ref.at[:, cols], out_hbm.at[:, cols], sems.at[n]))
+            copies[-1].start()
+        for copy in copies:
+            copy.wait()
+
+    return pl.pallas_call(
+        kernel,
+        in_specs=[ONCHIP, ONCHIP],
+        out_specs=ANY,
         out_shape=jax.ShapeDtypeStruct((tok, half), BF16),
+        scratch_shapes=[pltpu.VMEM((tok, half), BF16), pltpu.SemaphoreType.DMA((half // block,))],
         cost_estimate=pl.CostEstimate(
             flops=2 * tok * rows * half, bytes_accessed=2 * (rows * (half + tok) + tok * half), transcendentals=0
         ),
@@ -237,13 +244,14 @@
     ends = [rows * n // PIECES_OF for n in PIECE_ENDS]
     starts = [0] + ends[:-1]
     others = [lax.ppermute(own[first:end], "tp", swap) for first, end in zip(starts, ends)]
-    hidden = [
-        hidden_units(core, own, other, norm_gain, w_gate, w_up, first, weights if first == 0 else None)
-        for first, other in zip(starts, others)
-    ]
-    crossed = [lax.ppermute(piece, "tp", swap) for piece in hidden]
-    result = first_down_rows(core, hidden[:-1], crossed[:-1], starts[:-1], w_down, rows)
-    result = last_down_rows(core, hidden[-1], crossed[-1], starts[-1], w_down, result)
+    product = lambda n, room, after, result: hidden_units(
+        core, own, others[n], norm_gain, w_gate, w_up, starts[n], room, after, result
+    )
+    early = product(1, ends[1], None, product(0, ends[1], weights, None))
+    late = product(2, rows - ends[1], None, None)
+    crossed = [lax.ppermute(piece, "tp", swap) for piece in (early, late)]
+    result = first_down_rows(core, [early], crossed[:1], [0], w_down, rows)
+    result = last_down_rows(core, late, crossed[1], ends[1], w_down, result)
     return combine(weights, exchange(result))
 
 

time: 199 us -> 199 us (level)
  transfers between devices with their start and end apart: 6 -> 5, of which waited for: 2 -> 1; matrix products, arithmetic and copies ran while one was open for 0% -> 0% of each run, Pallas kernels for 4% -> 4%
where the time goes in v6:
time: 199 us
  blocking collectives  180 us (90%)
  Pallas kernels  13 us (7%)
  local copies, waits for them, and re-layouts  2.25 us (1%)
    all_to_all x2, blocking collectives, exchange(): array = lax.all_to_all(array, 'ep', split_axis=0, concat_axis=0, tiled=True)  180 us
    pallas_call x3, Pallas kernels, hidden_units(): pl.pallas_call(kernel, grid=() if result is None else (1,), in_specs=[SCA...  5.15 us
  transfers between devices with their start and end apart: 5, of which 1 were waited for; matrix products, arithmetic and copies ran while one was open for 0% of the time, Pallas kernels for 4%

profile of v6, /device:TPU:646, one launch (start us, length us, event | category | flops | bytes accessed | tf_op | source)
XLA Modules:
  0.0 198.6 jit_solution(13760604706439734966)
XLA Ops:
  0.0 0.7 copy-done.4
  0.7 1.2 copy-done.7
  1.9 2.0 %select_rows.1 = bf16[1536,1024]{1,0:T(8,128)(2,1)S(1)} custom-call(s32[1]{0:T(128)} %bitcast.2.core_ref, s32[2,512]{1,0:T(2,128)S(1)} %bitcast.30, bf16[512,1024]{1,0:T(8,128)(2,1)S(1)} %copy-done.7), custom_call_target="tpu_custom_call" | custom-call | flops 1610612736 | bytes 4194304 | tf_op jit(solution)/shard_map/select_rows/pallas_call | solution.py:53
  3.9 95.4 %all_to_all.10 = bf16[64,24,1024]{2,1,0:T(8,128)(2,1)S(1)} all-to-all(bf16[64,24,1024]{2,1,0:T(8,128)(2,1)S(1)} %bitcast.26), channel_id=1, replica_groups=mesh['grp'=2,'ep'=64,'tp'=2] {'ep'}, dimensions={0} | all-to-all | bytes 6291456 | tf_op jit(solution)/shard_map/all_to_all | solution.py:239
  99.4 0.3 fusion
  99.7 0.0 copy-start
  99.7 0.0 copy-start.1
  99.7 0.0 copy-start.3
  99.7 0.1 collective-permute-start.3
  99.9 0.5 collective-permute-start.2
  100.3 0.1 collective-permute-start
  100.5 0.0 copy-done.5
  100.5 0.0 copy-done.6
  100.5 1.0 combine_matrix.1.rest_0_.weights_ref
  101.5 1.0 collective-permute-done.3.other_ref
  102.5 0.0 copy-done
  102.5 0.0 copy-done.1
  102.5 1.7 hidden_units.4.rest_0_
  104.2 0.0 collective-permute-done.2.other_ref
  104.2 1.7 hidden_units.5.rest_0_
  106.0 0.0 copy-start.2
  106.0 0.3 collective-permute-start.4
  106.2 0.0 collective-permute-done.other_ref
  106.2 1.7 hidden_units.3.own_ref
  108.0 0.7 collective-permute-start.1
  108.6 0.0 collective-permute-done.4.rest_1_
  108.7 0.0 copy-done.2
  108.7 1.3 first_down_rows.1.result_ref
  109.9 0.0 collective-permute-done.1.other_ref
  109.9 0.9 last_down_rows.1
  110.9 84.9 %all_to_all.11 = bf16[64,24,1024]{2,1,0:T(8,128)(2,1)S(1)} all-to-all(bf16[64,24,1024]{2,1,0:T(8,128)(2,1)S(1)} %bitcast.16), channel_id=1, replica_groups=mesh['grp'=2,'ep'=64,'tp'=2] {'ep'}, dimensions={0} | all-to-all | bytes 6291456 | tf_op jit(solution)/shard_map/all_to_all | solution.py:239
  195.8 2.7 %combine.1 = bf16[512,1024]{1,0:T(8,128)(2,1)} custom-call(bf16[512,1536]{1,0:T(8,128)(2,1)S(1)} %combine_matrix.1.rest_0_.weights_ref, bf16[1536,1024]{1,0:T(8,128)(2,1)S(1)} %bitcast.25), custom_call_target="tpu_custom_call" | custom-call | flops 1610612736 | bytes 5767168 | tf_op jit(solution)/shard_map/combine/pallas_call | solution.py:214
  (5 shorter events, 0.0 us)
Async XLA Ops:
  0.0 0.7 copy-start.4
  0.7 1.2 copy-start.7
  99.4 1.1 copy-start.5
  99.4 1.1 copy-start.6
  99.7 2.8 %copy-start = (bf16[1,2048,256]{2,1,0:T(8,128)(2,1)S(1)}, bf16[1,2048,256]{2,1,0:T(8,128)(2,1)}, u32[]{:S(2)}) copy-start(bf16[1,2048,256]{2,1,0:T(8,128)(2,1)} %param.11) | copy-start | bytes 3145732
  99.7 2.8 %copy-start.1 = (bf16[1,2048,256]{2,1,0:T(8,128)(2,1)S(1)}, bf16[1,2048,256]{2,1,0:T(8,128)(2,1)}, u32[]{:S(2)}) copy-start(bf16[1,2048,256]{2,1,0:T(8,128)(2,1)} %param.12) | copy-start | bytes 3145732
  99.7 2.8 %copy-start.3 = (f32[2048]{0:T(1024)S(1)}, f32[2048]{0:T(1024)}, u32[]{:S(2)}) copy-start(f32[2048]{0:T(1024)} %param.8) | copy-start | bytes 24580
  99.7 2.8 %collective-permute-start.3 = (bf16[512,1024]{1,0:T(8,128)(2,1)S(1)}, bf16[512,1024]{1,0:T(8,128)(2,1)S(1)}, u32[]{:S(2)}, u32[]{:S(2)}) collective-permute-start(bf16[512,1024]{1,0:T(8,128)(2,1)S(1)} %get-tuple-element.5), channel_id=1, source_target_pairs={{0,1},{1,0},{2,3},{3,2},{4,5},{5,4},{6,7},{7,6},{8,9},{9,8},{10,11... | collective-permute-start | bytes 3145736 | tf_op jit(solution)/shard_map/ppermute | solution.py:246
  99.9 4.4 %collective-permute-start.2 = (bf16[512,1024]{1,0:T(8,128)(2,1)S(1)}, bf16[512,1024]{1,0:T(8,128)(2,1)S(1)}, u32[]{:S(2)}, u32[]{:S(2)}) collective-permute-start(bf16[512,1024]{1,0:T(8,128)(2,1)S(1)} %get-tuple-element.6), channel_id=1, source_target_pairs={{0,1},{1,0},{2,3},{3,2},{4,5},{5,4},{6,7},{7,6},{8,9},{9,8},{10,11... | collective-permute-start | bytes 3145736 | tf_op jit(solution)/shard_map/ppermute | solution.py:246
  100.3 5.9 %collective-permute-start = (bf16[512,1024]{1,0:T(8,128)(2,1)S(1)}, bf16[512,1024]{1,0:T(8,128)(2,1)S(1)}, u32[]{:S(2)}, u32[]{:S(2)}) collective-permute-start(bf16[512,1024]{1,0:T(8,128)(2,1)S(1)} %get-tuple-element.7), channel_id=1, source_target_pairs={{0,1},{1,0},{2,3},{3,2},{4,5},{5,4},{6,7},{7,6},{8,9},{9,8},{10,11... | collective-permute-start | bytes 3145736 | tf_op jit(solution)/shard_map/ppermute | solution.py:246
  106.0 2.7 %copy-start.2 = (bf16[1,512,1024]{2,1,0:T(8,128)(2,1)S(1)}, bf16[1,512,1024]{2,1,0:T(8,128)(2,1)}, u32[]{:S(2)}) copy-start(bf16[1,512,1024]{2,1,0:T(8,128)(2,1)} %param.13) | copy-start | bytes 3145732
  106.0 2.7 %collective-permute-start.4 = (bf16[1024,256]{1,0:T(8,128)(2,1)S(1)}, bf16[1024,256]{1,0:T(8,128)(2,1)S(1)}, u32[]{:S(2)}, u32[]{:S(2)}) collective-permute-start(bf16[1024,256]{1,0:T(8,128)(2,1)S(1)} %hidden_units.5.rest_0_), channel_id=1, source_target_pairs={{0,1},{1,0},{2,3},{3,2},{4,5},{5,4},{6,7},{7,6},{8,9},{9,8},{10,11... | collective-permute-start | bytes 1572872 | tf_op jit(solution)/shard_map/ppermute | solution.py:252
  108.0 2.0 collective-permute-start.1

commit v7 on v6

--- a/solution.py
+++ b/solution.py
@@ -172,20 +172,20 @@
     rows, units = own.shape
     total, half = result.shape
     block = block_of(rows, 256)
-    skip = first // block
 
     def kernel(core_ref, own_ref, other_ref, w_ref, result_ref, out_ref):
         mine = core_ref[0]
-        part = pl.ds(pl.multiple_of(pl.program_id(0) * block, block), block)
-        out = jnp.dot(own_ref[part, :], w_ref[mine], preferred_element_type=F32)
-        out = out + jnp.dot(other_ref[part, :], w_ref[1 - mine], preferred_element_type=F32)
-        out_ref[...] = out.astype(BF16)
-
-    return pl.pallas_call(
-        kernel,
-        grid=(rows // block,),
+        for start in range(0, rows, block):
+            part = pl.ds(start, block)
+            out = jnp.dot(own_ref[part, :], w_ref[mine], preferred_element_type=F32)
+            out = out + jnp.dot(other_ref[part, :], w_ref[1 - mine], preferred_element_type=F32)
+            out_ref[part, :] = out.astype(BF16)
+
+    return pl.pallas_call(
+        kernel,
+        grid=(1,),
         in_specs=[SCALAR, ONCHIP, ONCHIP, ONCHIP, ANY],
-        out_specs=pl.BlockSpec((block, half), lambda i: (i + skip, 0)),
+        out_specs=pl.BlockSpec((rows, half), lambda i: (first // rows, 0)),
         out_shape=jax.ShapeDtypeStruct((total, half), BF16),
         input_output_aliases={4: 0},
         cost_estimate=pl.CostEstimate(

time: 199 us -> 199 us (level)
  no operation moved by 1% of the time
where the time goes in v7:
time: 199 us; the launch traced here: 198 us
  blocking collectives  180 us (90%)
  Pallas kernels  12.8 us (6%)
  local copies, waits for them, and re-layouts  2.25 us (1%)
    all_to_all x2, blocking collectives, exchange(): array = lax.all_to_all(array, 'ep', split_axis=0, concat_axis=0, tiled=True)  180 us
    pallas_call x3, Pallas kernels, hidden_units(): pl.pallas_call(kernel, grid=() if result is None else (1,), in_specs=[SCA...  5.15 us
  transfers between devices with their start and end apart: 5, of which 1 were waited for; matrix products, arithmetic and copies ran while one was open for 0% of the time, Pallas kernels for 4%

profile of v7, /device:TPU:646, one launch (start us, length us, event | category | flops | bytes accessed | tf_op | source)
XLA Modules:
  0.0 198.4 jit_solution(1309946758671114983)
XLA Ops:
  0.0 0.7 copy-done.4
  0.7 1.2 copy-done.7
  1.9 2.0 %select_rows.1 = bf16[1536,1024]{1,0:T(8,128)(2,1)S(1)} custom-call(s32[1]{0:T(128)} %bitcast.2.core_ref, s32[2,512]{1,0:T(2,128)S(1)} %bitcast.30, bf16[512,1024]{1,0:T(8,128)(2,1)S(1)} %copy-done.7), custom_call_target="tpu_custom_call" | custom-call | flops 1610612736 | bytes 4194304 | tf_op jit(solution)/shard_map/select_rows/pallas_call | solution.py:53
  3.9 95.4 %all_to_all.10 = bf16[64,24,1024]{2,1,0:T(8,128)(2,1)S(1)} all-to-all(bf16[64,24,1024]{2,1,0:T(8,128)(2,1)S(1)} %bitcast.26), channel_id=1, replica_groups=mesh['grp'=2,'ep'=64,'tp'=2] {'ep'}, dimensions={0} | all-to-all | bytes 6291456 | tf_op jit(solution)/shard_map/all_to_all | solution.py:239
  99.4 0.3 fusion
  99.7 0.0 copy-start
  99.7 0.0 copy-start.1
  99.7 0.0 copy-start.3
  99.7 0.1 collective-permute-start.3
  99.9 0.5 collective-permute-start.2
  100.3 0.1 collective-permute-start
  100.5 0.0 copy-done.5
  100.5 0.0 copy-done.6
  100.5 1.0 combine_matrix.1.rest_0_.weights_ref
  101.5 1.0 collective-permute-done.3.other_ref
  102.5 0.0 copy-done
  102.5 0.0 copy-done.1
  102.5 1.7 hidden_units.4.rest_0_
  104.2 0.0 collective-permute-done.2.other_ref
  104.2 1.7 hidden_units.5.rest_0_
  106.0 0.0 copy-start.2
  106.0 0.3 collective-permute-start.4
  106.2 0.0 collective-permute-done.other_ref
  106.2 1.7 hidden_units.3.own_ref
  108.0 0.7 collective-permute-start.1
  108.6 0.0 collective-permute-done.4.rest_1_
  108.7 0.0 copy-done.2
  108.7 1.3 first_down_rows.1.result_ref
  109.9 0.0 collective-permute-done.1.other_ref
  109.9 0.7 last_down_rows.1
  110.7 84.9 %all_to_all.11 = bf16[64,24,1024]{2,1,0:T(8,128)(2,1)S(1)} all-to-all(bf16[64,24,1024]{2,1,0:T(8,128)(2,1)S(1)} %bitcast.16), channel_id=1, replica_groups=mesh['grp'=2,'ep'=64,'tp'=2] {'ep'}, dimensions={0} | all-to-all | bytes 6291456 | tf_op jit(solution)/shard_map/all_to_all | solution.py:239
  195.5 2.7 %combine.1 = bf16[512,1024]{1,0:T(8,128)(2,1)} custom-call(bf16[512,1536]{1,0:T(8,128)(2,1)S(1)} %combine_matrix.1.rest_0_.weights_ref, bf16[1536,1024]{1,0:T(8,128)(2,1)S(1)} %bitcast.25), custom_call_target="tpu_custom_call" | custom-call | flops 1610612736 | bytes 5767168 | tf_op jit(solution)/shard_map/combine/pallas_call | solution.py:214
  (5 shorter events, 0.0 us)
Async XLA Ops:
  0.0 0.7 copy-start.4
  0.7 1.2 copy-start.7
  99.4 1.1 copy-start.5
  99.4 1.1 copy-start.6
  99.7 2.8 %copy-start = (bf16[1,2048,256]{2,1,0:T(8,128)(2,1)S(1)}, bf16[1,2048,256]{2,1,0:T(8,128)(2,1)}, u32[]{:S(2)}) copy-start(bf16[1,2048,256]{2,1,0:T(8,128)(2,1)} %param.11) | copy-start | bytes 3145732
  99.7 2.8 %copy-start.1 = (bf16[1,2048,256]{2,1,0:T(8,128)(2,1)S(1)}, bf16[1,2048,256]{2,1,0:T(8,128)(2,1)}, u32[]{:S(2)}) copy-start(bf16[1,2048,256]{2,1,0:T(8,128)(2,1)} %param.12) | copy-start | bytes 3145732
  99.7 2.8 %copy-start.3 = (f32[2048]{0:T(1024)S(1)}, f32[2048]{0:T(1024)}, u32[]{:S(2)}) copy-start(f32[2048]{0:T(1024)} %param.8) | copy-start | bytes 24580
  99.7 2.8 %collective-permute-start.3 = (bf16[512,1024]{1,0:T(8,128)(2,1)S(1)}, bf16[512,1024]{1,0:T(8,128)(2,1)S(1)}, u32[]{:S(2)}, u32[]{:S(2)}) collective-permute-start(bf16[512,1024]{1,0:T(8,128)(2,1)S(1)} %get-tuple-element.5), channel_id=1, source_target_pairs={{0,1},{1,0},{2,3},{3,2},{4,5},{5,4},{6,7},{7,6},{8,9},{9,8},{10,11... | collective-permute-start | bytes 3145736 | tf_op jit(solution)/shard_map/ppermute | solution.py:246
  99.9 4.4 %collective-permute-start.2 = (bf16[512,1024]{1,0:T(8,128)(2,1)S(1)}, bf16[512,1024]{1,0:T(8,128)(2,1)S(1)}, u32[]{:S(2)}, u32[]{:S(2)}) collective-permute-start(bf16[512,1024]{1,0:T(8,128)(2,1)S(1)} %get-tuple-element.6), channel_id=1, source_target_pairs={{0,1},{1,0},{2,3},{3,2},{4,5},{5,4},{6,7},{7,6},{8,9},{9,8},{10,11... | collective-permute-start | bytes 3145736 | tf_op jit(solution)/shard_map/ppermute | solution.py:246
  100.3 5.9 %collective-permute-start = (bf16[512,1024]{1,0:T(8,128)(2,1)S(1)}, bf16[512,1024]{1,0:T(8,128)(2,1)S(1)}, u32[]{:S(2)}, u32[]{:S(2)}) collective-permute-start(bf16[512,1024]{1,0:T(8,128)(2,1)S(1)} %get-tuple-element.7), channel_id=1, source_target_pairs={{0,1},{1,0},{2,3},{3,2},{4,5},{5,4},{6,7},{7,6},{8,9},{9,8},{10,11... | collective-permute-start | bytes 3145736 | tf_op jit(solution)/shard_map/ppermute | solution.py:246
  106.0 2.7 %copy-start.2 = (bf16[1,512,1024]{2,1,0:T(8,128)(2,1)S(1)}, bf16[1,512,1024]{2,1,0:T(8,128)(2,1)}, u32[]{:S(2)}) copy-start(bf16[1,512,1024]{2,1,0:T(8,128)(2,1)} %param.13) | copy-start | bytes 3145732
  106.0 2.7 %collective-permute-start.4 = (bf16[1024,256]{1,0:T(8,128)(2,1)S(1)}, bf16[1024,256]{1,0:T(8,128)(2,1)S(1)}, u32[]{:S(2)}, u32[]{:S(2)}) collective-permute-start(bf16[1024,256]{1,0:T(8,128)(2,1)S(1)} %hidden_units.5.rest_0_), channel_id=1, source_target_pairs={{0,1},{1,0},{2,3},{3,2},{4,5},{5,4},{6,7},{7,6},{8,9},{9,8},{10,11... | collective-permute-start | bytes 1572872 | tf_op jit(solution)/shard_map/ppermute | solution.py:252
  108.0 2.0 collective-permute-start.1
